TPU v7x, 32 devices: a whole 2x2x4 slice. The times are simulated.
32 devices in a mesh: gr: 2 (over x), fs: 4 (over z), tp: 4 (over y, core).
Axes of the slice: x: 2, y: 2, z: 4, core: 2. Of those that a mesh axis runs over, the one named last changes fastest.
Arguments:
- prompt: bfloat16 [4096, 2048], P(('gr', 'fs')), may hold values from -6 to 6
- gain_first: float32 [2048], P(('gr', 'fs')), may hold values from 0.1 to 1.9
- gate_first: float32 [2048, 2816], P(('gr', 'fs'), 'tp'), may hold values from -0.125 to 0.125
- up_first: float32 [2048, 2816], P(('gr', 'fs'), 'tp'), may hold values from -0.125 to 0.125
- down_first: float32 [2816, 2048], P(('gr', 'fs'), 'tp'), may hold values from -0.109375 to 0.109375
- gain_second: float32 [2048], P(('gr', 'fs')), may hold values from 0.1 to 1.9
- gate_second: float32 [2048, 2816], P(('gr', 'fs'), 'tp'), may hold values from -0.125 to 0.125
- up_second: float32 [2048, 2816], P(('gr', 'fs'), 'tp'), may hold values from -0.125 to 0.125
- down_second: float32 [2816, 2048], P(('gr', 'fs'), 'tp'), may hold values from -0.109375 to 0.109375
Outputs:
- serve_gate_first: bfloat16 [2048, 2816], P(None, 'tp')
- serve_up_first: bfloat16 [2048, 2816], P(None, 'tp')
- serve_down_first: bfloat16 [2816, 2048], P('tp')
- serve_gate_second: bfloat16 [2048, 2816], P(None, 'tp')
- serve_up_second: bfloat16 [2048, 2816], P(None, 'tp')
- serve_down_second: bfloat16 [2816, 2048], P('tp')
- mixed: bfloat16 [4096, 2048], P(('gr', 'fs', 'tp'))
All inputs are finite; a program needn't handle non-finite values.
Results may differ from a plain program's by a relative error of at most 0.0085.
Values may be sent and summed in bfloat16 or wider, within the bound.
A program may use at most 128 MiB of HBM per device.

v0:
```python
import functools

import jax
import jax.numpy as jnp
from jax import lax
from jax.experimental import pallas as pl
from jax.experimental.pallas import tpu as pltpu
from jax.sharding import PartitionSpec as P

MESH = pl.DeviceIdType.MESH


def gather_kernel(
    n_gr,
    n_fs,
    n_tp,
    gain_ref,
    gate_ref,
    up_ref,
    down_ref,
    gate_out,
    up_out,
    down_out,
    down_own,
    line_send,
    line_recv,
    pair_send,
    pair_recv,
    part_send,
    part_recv,
):
    g, f, t = lax.axis_index("gr"), lax.axis_index("fs"), lax.axis_index("tp")
    per = n_gr * n_fs // n_tp
    cols = down_ref.shape[1]
    first = lax.rem(t * per, n_fs)
    home = (t * per) // n_fs
    row = g * n_fs + f
    owner = row // per
    slot = lax.rem(row, per)

    width = gate_ref.shape[1]

    def place(ref, origin):
        if len(ref.shape) == 3:
            return ref.at[origin]
        return ref.at[:, pl.ds(pl.multiple_of(origin * width, 128), width)]

    gain = gain_ref[...]
    place(gate_out, row)[...] = (gain * gate_ref[...]).astype(jnp.bfloat16)
    place(up_out, row)[...] = (gain * up_ref[...]).astype(jnp.bfloat16)
    down_own[...] = down_ref[...].astype(jnp.bfloat16)

    @pl.when(owner == t)
    def _():
        down_out[slot, :, pl.ds(pl.multiple_of(t * cols, 128), cols)] = down_ref[...].astype(
            jnp.bfloat16
        )

    barrier = pltpu.get_barrier_semaphore()
    for dg in range(n_gr):
        for dt in range(n_tp):
            if dg or dt:
                pl.semaphore_signal(
                    barrier,
                    inc=1,
                    device_id=(lax.rem(g + dg, n_gr), f, lax.rem(t + dt, n_tp)),
                    device_id_type=MESH,
                )

    for near in (lax.rem(f + 1, n_fs), lax.rem(f + n_fs - 1, n_fs)):
        pl.semaphore_signal(barrier, inc=1, device_id=(g, near, t), device_id_type=MESH)
    pl.semaphore_wait(barrier, n_gr * n_tp + 1)

    outs = (gate_out, up_out)

    def held(o):
        return jnp.logical_and(o >= first, o < first + per)

    def block(m, o):
        if m < 2:
            return place(outs[m], g * n_fs + o)
        return down_out.at[o - first]

    def line(m, way, s):
        step = 1 if way == 0 else -1
        o = f - step * (s - 1)
        return pltpu.make_async_remote_copy(
            src_ref=block(m, o),
            dst_ref=block(m, o),
            send_sem=line_send.at[m, way, s],
            recv_sem=line_recv.at[m, way, s],
            device_id=(g, f + step, t),
            device_id_type=MESH,
        )

    def sends(m, way, s):
        step = 1 if way == 0 else -1
        o = f - step * (s - 1)
        fine = (f < n_fs - 1, o >= 0) if way == 0 else (f > 0, o <= n_fs - 1)
        ok = jnp.logical_and(*fine)
        return jnp.logical_and(ok, held(o)) if m == 2 else ok

    def gets(m, way, s):
        o = f - s if way == 0 else f + s
        ok = o >= 0 if way == 0 else o <= n_fs - 1
        return jnp.logical_and(ok, held(o)) if m == 2 else ok

    def landed(m, way, s):
        o = f - s if way == 0 else f + s
        return pltpu.make_async_remote_copy(
            src_ref=block(m, o),
            dst_ref=block(m, o),
            send_sem=line_send.at[m, way, s],
            recv_sem=line_recv.at[m, way, s],
            device_id=(g, f, t),
            device_id_type=MESH,
        )

    def pair(m, dg, o):
        return pltpu.make_async_remote_copy(
            src_ref=place(outs[m], g * n_fs + o),
            dst_ref=place(outs[m], g * n_fs + o),
            send_sem=pair_send.at[m, dg, o],
            recv_sem=pair_recv.at[m, dg, o],
            device_id=(lax.rem(g + dg, n_gr), f, t),
            device_id_type=MESH,
        )

    def pair_landed(m, dg, o):
        src = lax.rem(g - dg + n_gr, n_gr)
        return pltpu.make_async_remote_copy(
            src_ref=place(outs[m], src * n_fs + o),
            dst_ref=place(outs[m], src * n_fs + o),
            send_sem=pair_send.at[m, dg, o],
            recv_sem=pair_recv.at[m, dg, o],
            device_id=(src, f, t),
            device_id_type=MESH,
        )

    def part(dg):
        to = lax.rem(g + dg, n_gr)
        return pltpu.make_async_remote_copy(
            src_ref=down_own,
            dst_ref=down_out.at[slot, :, pl.ds(pl.multiple_of(t * cols, 128), cols)],
            send_sem=part_send.at[dg],
            recv_sem=part_recv.at[t],
            device_id=(to, f, owner),
            device_id_type=MESH,
        )

    def part_landed(src):
        return pltpu.make_async_remote_copy(
            src_ref=down_own,
            dst_ref=down_out.at[f - first, :, pl.ds(src * cols, cols)],
            send_sem=part_send.at[0],
            recv_sem=part_recv.at[src],
            device_id=(home, f, src),
            device_id_type=MESH,
        )

    for m in range(2):
        for way in range(2):

            @pl.when(sends(m, way, 1))
            def _(m=m, way=way):
                line(m, way, 1).start()

        for dg in range(1, n_gr):
            pair(m, dg, f).start()
    for dg in range(n_gr):
        if dg == 0:

            @pl.when(owner != t)
            def _():
                part(0).start()

        else:
            part(dg).start()

    @pl.when(held(f))
    def _():
        for src in range(n_tp):

            @pl.when(jnp.logical_or(home != g, t != src))
            def _(src=src):
                part_landed(src).wait_recv()

    for way in range(2):

        @pl.when(sends(2, way, 1))
        def _(way=way):
            line(2, way, 1).start()

    for s in range(1, n_fs):
        for m in range(3):
            for way in range(2):

                @pl.when(gets(m, way, s))
                def _(m=m, way=way, s=s):
                    landed(m, way, s).wait_recv()
                    if s < n_fs - 1:

                        @pl.when(sends(m, way, s + 1))
                        def _():
                            line(m, way, s + 1).start()

                    if m < 2:
                        o = f - s if way == 0 else f + s
                        for dg in range(1, n_gr):
                            pair(m, dg, o).start()

    for m in range(2):
        for dg in range(1, n_gr):
            for o in range(n_fs):
                pair_landed(m, dg, o).wait_recv()
                pair(m, dg, o).wait_send()
    for m in range(3):
        for way in range(2):
            for s in range(1, n_fs):

                @pl.when(sends(m, way, s))
                def _(m=m, way=way, s=s):
                    line(m, way, s).wait_send()

    for dg in range(n_gr):
        if dg == 0:

            @pl.when(owner != t)
            def _():
                part(0).wait_send()

        else:
            part(dg).wait_send()


def gather(sizes, call, gain, gate, up, down):
    n_gr, n_fs, n_tp = sizes
    per = n_gr * n_fs // n_tp
    rows, width = gate.shape
    wide = rows % 128 == 0
    whole = (width, n_gr * n_fs * rows) if wide else (n_gr * n_fs, width, rows)
    tall, cols = down.shape
    vmem = pl.BlockSpec(memory_space=pltpu.VMEM)
    dma = pltpu.SemaphoreType.DMA
    gate_all, up_all, down_all = pl.pallas_call(
        functools.partial(gather_kernel, n_gr, n_fs, n_tp),
        out_shape=(
            jax.ShapeDtypeStruct(whole, jnp.bfloat16),
            jax.ShapeDtypeStruct(whole, jnp.bfloat16),
            jax.ShapeDtypeStruct((per, tall, n_tp * cols), jnp.bfloat16),
        ),
        in_specs=[vmem] * 4,
        out_specs=(vmem,) * 3,
        scratch_shapes=[
            pltpu.VMEM((tall, cols), jnp.bfloat16),
            dma((3, 2, n_fs)),
            dma((3, 2, n_fs)),
            dma((2, n_gr, n_fs)),
            dma((2, n_gr, n_fs)),
            dma((n_gr,)),
            dma((n_tp,)),
        ],
        compiler_params=pltpu.CompilerParams(
            collective_id=call, has_side_effects=True, vmem_limit_bytes=32 * 2**20
        ),
        cost_estimate=pl.CostEstimate(
            flops=10**10, bytes_accessed=16 * 2**20, transcendentals=0
        ),
    )(gain[None, :], gate.T, up.T, down)

    def upright(a):
        return a.T if wide else a.transpose(0, 2, 1).reshape(n_gr * n_fs * rows, width)

    return (
        upright(gate_all),
        upright(up_all),
        down_all.reshape(per * tall, n_tp * cols),
    )


def fused_kernel(
    n_gr,
    n_fs,
    n_tp,
    prompt_ref,
    gain_a,
    gate_a,
    up_a,
    down_a,
    gain_b,
    gate_b,
    up_b,
    down_b,
    gate_out_a,
    up_out_a,
    down_out_a,
    gate_out_b,
    up_out_b,
    down_out_b,
    mixed_ref,
    down_own,
    normed,
    normed_all,
    hidden,
    parts,
    mate_in,
    sums,
    parts_in,
    kept,
    stream,
    line_send,
    line_recv,
    pair_send,
    pair_recv,
    part_send,
    part_recv,
    mate_send,
    mate_recv,
    sum_send,
    sum_recv,
    row_send,
    row_recv,
):
    g, f, t = lax.axis_index("gr"), lax.axis_index("fs"), lax.axis_index("tp")
    per = n_gr * n_fs // n_tp
    cols = down_a.shape[1]
    width = gate_a.shape[1]
    first = lax.rem(t * per, n_fs)
    home = (t * per) // n_fs
    row = g * n_fs + f
    owner = row // per
    slot = lax.rem(row, per)
    half = n_tp * cols // n_gr
    lane = t * n_gr // n_tp
    outs = ((gate_out_a, up_out_a, down_out_a), (gate_out_b, up_out_b, down_out_b))

    def halved(n):
        return n == 1

    def place(ref, origin):
        return ref.at[:, pl.ds(pl.multiple_of(origin * width, 128), width)]

    for n, (gain, gate, up, down) in enumerate(
        ((gain_a, gate_a, up_a, down_a), (gain_b, gate_b, up_b, down_b))
    ):
        place(outs[n][0], row)[...] = (gain[...] * gate[...]).astype(jnp.bfloat16)
        place(outs[n][1], row)[...] = (gain[...] * up[...]).astype(jnp.bfloat16)
        down_own[n] = down[...].astype(jnp.bfloat16)

        @pl.when(jnp.logical_and(owner == t, lane == g) if halved(n) else owner == t)
        def _(n=n, down=down):
            outs[n][2][slot, :, pl.ds(pl.multiple_of(t * cols, 128), cols)] = down[...].astype(
                jnp.bfloat16
            )

    barrier = pltpu.get_barrier_semaphore()
    for dg in range(n_gr):
        for dt in range(n_tp):
            if dg or dt:
                pl.semaphore_signal(
                    barrier,
                    inc=1,
                    device_id=(lax.rem(g + dg, n_gr), f, lax.rem(t + dt, n_tp)),
                    device_id_type=MESH,
                )
    for near in (lax.rem(f + 1, n_fs), lax.rem(f + n_fs - 1, n_fs)):
        pl.semaphore_signal(barrier, inc=1, device_id=(g, near, t), device_id_type=MESH)
    pl.semaphore_wait(barrier, n_gr * n_tp + 1)

    def held(o):
        return jnp.logical_and(o >= first, o < first + per)

    def remote(src, dst, send, recv, to):
        return pltpu.make_async_remote_copy(
            src_ref=src,
            dst_ref=dst,
            send_sem=send,
            recv_sem=recv,
            device_id=to,
            device_id_type=MESH,
        )

    def block(n, m, o):
        if m < 2:
            return place(outs[n][m], g * n_fs + o)
        if halved(n):
            return share_of(n, o, g)
        return outs[n][2].at[o - first]

    def share_of(n, o, column):
        return outs[n][2].at[o - first, :, pl.ds(pl.multiple_of(column * half, 128), half)]

    def line(n, m, way, s):
        step = 1 if way == 0 else -1
        o = f - step * (s - 1)
        sems = line_send.at[n, m, way, s], line_recv.at[n, m, way, s]
        return remote(block(n, m, o), block(n, m, o), *sems, (g, f + step, t))

    def sends(m, way, s):
        step = 1 if way == 0 else -1
        o = f - step * (s - 1)
        fine = (f < n_fs - 1, o >= 0) if way == 0 else (f > 0, o <= n_fs - 1)
        ok = jnp.logical_and(*fine)
        return jnp.logical_and(ok, held(o)) if m == 2 else ok

    def gets(m, way, s):
        o = f - s if way == 0 else f + s
        ok = o >= 0 if way == 0 else o <= n_fs - 1
        return jnp.logical_and(ok, held(o)) if m == 2 else ok

    def landed(n, m, way, s):
        o = f - s if way == 0 else f + s
        sems = line_send.at[n, m, way, s], line_recv.at[n, m, way, s]
        return remote(block(n, m, o), block(n, m, o), *sems, (g, f, t))

    def pair(n, m, dg, o):
        spot = share_of(n, o, g) if m == 2 else place(outs[n][m], g * n_fs + o)
        sems = pair_send.at[n, m, dg, o], pair_recv.at[n, m, dg, o]
        return remote(spot, spot, *sems, (lax.rem(g + dg, n_gr), f, t))

    def pair_landed(n, m, dg, o):
        src = lax.rem(g - dg + n_gr, n_gr)
        spot = share_of(n, o, src) if m == 2 else place(outs[n][m], src * n_fs + o)
        sems = pair_send.at[n, m, dg, o], pair_recv.at[n, m, dg, o]
        return remote(spot, spot, *sems, (src, f, t))

    def part(n, dg):
        return remote(
            down_own.at[n],
            outs[n][2].at[slot, :, pl.ds(pl.multiple_of(t * cols, 128), cols)],
            part_send.at[n, dg],
            part_recv.at[n, t],
            (lane if halved(n) else lax.rem(g + dg, n_gr), f, owner),
        )

    def part_landed(n, src):
        return remote(
            down_own.at[n],
            outs[n][2].at[f - first, :, pl.ds(src * cols, cols)],
            part_send.at[n, 0],
            part_recv.at[n, src],
            (home, f, src),
        )

    def start_own(n):
        for m in range(2):
            for way in range(2):

                @pl.when(sends(m, way, 1))
                def _(m=m, way=way):
                    line(n, m, way, 1).start()

            for dg in range(1, n_gr):
                pair(n, m, dg, f).start()
        for dg in range(n_gr):
            if halved(n):
                if dg == 0:

                    @pl.when(jnp.logical_or(owner != t, lane != g))
                    def _():
                        part(n, 0).start()

            elif dg == 0:

                @pl.when(owner != t)
                def _():
                    part(n, 0).start()

            else:
                part(n, dg).start()

    def start_down(n):
        @pl.when(held(f))
        def _():
            for src in range(n_tp):

                away = jnp.logical_or(home != g, t != src)
                if halved(n):
                    away = jnp.logical_and(away, g == src * n_gr // n_tp)

                @pl.when(away)
                def _(src=src):
                    part_landed(n, src).wait_recv()

            if halved(n):
                for dg in range(1, n_gr):
                    pair(n, 2, dg, f).start()

        for way in range(2):

            @pl.when(sends(2, way, 1))
            def _(way=way):
                line(n, 2, way, 1).start()

    def forward(n, m, s):
        for way in range(2):

            @pl.when(gets(m, way, s))
            def _(way=way):
                landed(n, m, way, s).wait_recv()
                if s < n_fs - 1:

                    @pl.when(sends(m, way, s + 1))
                    def _():
                        line(n, m, way, s + 1).start()

                if m < 2 or halved(n):
                    o = f - s if way == 0 else f + s
                    for dg in range(1, n_gr):
                        pair(n, m, dg, o).start()

    def pairs_in(n):
        for m in range(2):
            for dg in range(1, n_gr):
                for o in range(n_fs):
                    pair_landed(n, m, dg, o).wait_recv()

    def halves(n, act):
        for dg in range(1, n_gr):
            for o in range(n_fs):

                @pl.when(held(o))
                def _(dg=dg, o=o):
                    act(n, 2, dg, o)

    def drain(n):
        if halved(n):
            halves(n, lambda *at: pair(*at).wait_send())
        for m in range(2):
            for dg in range(1, n_gr):
                for o in range(n_fs):
                    pair(n, m, dg, o).wait_send()
        for m in range(3):
            for way in range(2):
                for s in range(1, n_fs):

                    @pl.when(sends(m, way, s))
                    def _(m=m, way=way, s=s):
                        line(n, m, way, s).wait_send()

        for dg in range(n_gr):
            if halved(n):
                if dg == 0:

                    @pl.when(jnp.logical_or(owner != t, lane != g))
                    def _():
                        part(n, 0).wait_send()

            elif dg == 0:

                @pl.when(owner != t)
                def _():
                    part(n, 0).wait_send()

            else:
                part(n, dg).wait_send()

    owned, depth = prompt_ref.shape[1], prompt_ref.shape[2]
    across = (((1,), (1,)), ((), ()))

    def unit(rows):
        return rows * lax.rsqrt(jnp.mean(rows * rows, axis=-1, keepdims=True) + 1e-06)

    def hide(n, source):
        @pl.loop(0, n_tp // 2)
        def _(i):
            rows = source[pl.ds(2 * i, 2)].reshape(2 * owned, depth)
            gate = lax.dot_general(
                rows, outs[n][0][...], across, preferred_element_type=jnp.float32
            )
            upper = lax.dot_general(
                rows, outs[n][1][...], across, preferred_element_type=jnp.float32
            )
            units = (jax.nn.silu(gate) * upper).astype(jnp.bfloat16)
            hidden[pl.ds(2 * i, 2)] = units.reshape(2, owned, units.shape[1])

    pairs = n_tp // 2
    seat, core = t // 2, lax.rem(t, 2)

    def at_seat(j):
        return 2 * lax.rem(seat + 1 + j, pairs)

    def mate(n, j):
        return remote(
            parts.at[n, j],
            mate_in.at[n, j],
            mate_send.at[n, j],
            mate_recv.at[n, j],
            (g, f, t + 1 - 2 * core),
        )

    def share(n, j):
        return remote(
            sums.at[n, j],
            parts_in.at[n, j],
            sum_send.at[n, j],
            sum_recv.at[n, j],
            (g, f, at_seat(j) + core),
        )

    def term(n, units):
        tall = outs[n][2].shape[1]
        total = jnp.zeros((owned, depth), jnp.float32)
        for k in range(per):
            total += jnp.dot(
                units[:, k * tall : (k + 1) * tall],
                outs[n][2][k],
                preferred_element_type=jnp.float32,
            )
        return total.astype(jnp.bfloat16)

    def spread(n):
        for j in range(pairs):
            parts[n, j] = term(n, hidden[at_seat(j) + 1 - core])
            if j > 0:
                mate(n, j - 1).start()
        for j in range(pairs):
            mine = term(n, hidden[at_seat(j) + core]).astype(jnp.float32)
            if j == 0:
                mate(n, pairs - 1).start()
            mate(n, j).wait_recv()
            both = mine + mate_in[n, j].astype(jnp.float32)
            if j < pairs - 1:
                sums[n, j] = both.astype(jnp.bfloat16)
                share(n, j).start()
            else:
                kept[...] = both

    def collect(n):
        total = kept[...]
        for j in range(pairs - 1):
            share(n, j).wait_recv()
            total += parts_in[n, j].astype(jnp.float32)
        return total

    def give(i):
        to = lax.rem(t + 1 + i, n_tp)
        return remote(
            normed_all.at[t], normed_all.at[t], row_send.at[i], row_recv.at[i], (g, f, to)
        )

    def given(i):
        src = lax.rem(t - 1 - i + n_tp, n_tp)
        return remote(
            normed_all.at[src], normed_all.at[src], row_send.at[i], row_recv.at[i], (g, f, src)
        )

    start_own(0)

    @pl.loop(0, n_tp)
    def _(i):
        normed[i] = unit(prompt_ref[i].astype(jnp.float32)).astype(jnp.bfloat16)

    start_down(0)
    for m in range(3):
        forward(0, m, 1)
    start_own(1)
    for s in range(2, n_fs):
        for m in range(3):
            forward(0, m, s)
    start_down(1)
    for m in range(3):
        forward(1, m, 1)
    pairs_in(0)
    hide(0, normed)
    spread(0)
    for s in range(2, n_fs - 1):
        for m in range(3):
            forward(1, m, s)
    stream[...] = prompt_ref[t].astype(jnp.float32) + 0.5 * collect(0)
    normed_all[t] = unit(stream[...]).astype(jnp.bfloat16)
    for m in range(2):
        forward(1, m, n_fs - 1)
    for i in range(n_tp - 1):
        give(i).start()
    for i in range(n_tp - 1):
        given(i).wait_recv()
    pairs_in(1)
    forward(1, 2, n_fs - 1)
    hide(1, normed_all)
    halves(1, lambda *at: pair_landed(*at).wait_recv())
    spread(1)
    drain(0)
    drain(1)
    mixed_ref[...] = (stream[...] + 0.5 * collect(1)).astype(jnp.bfloat16)
    for i in range(n_tp - 1):
        give(i).wait_send()
    for n in range(2):
        for j in range(pairs):
            mate(n, j).wait_send()
            if j < pairs - 1:
                share(n, j).wait_send()


def fused(sizes, prompt, *weights):
    n_gr, n_fs, n_tp = sizes
    per = n_gr * n_fs // n_tp
    tokens, depth = prompt.shape
    owned = tokens // n_tp
    rows, width = weights[1].shape
    tall, cols = weights[3].shape
    vmem = pl.BlockSpec(memory_space=pltpu.VMEM)
    dma = pltpu.SemaphoreType.DMA
    across = pltpu.VMEM((width, n_gr * n_fs * rows), jnp.bfloat16)
    down = pltpu.VMEM((per, tall, n_tp * cols), jnp.bfloat16)
    operands = [prompt.reshape(n_tp, owned, depth)]
    for n in range(2):
        gain, gate, up, tall_block = weights[4 * n : 4 * n + 4]
        operands += [gain[None, :], gate.T, up.T, tall_block]
    *served, mixed = pl.pallas_call(
        functools.partial(fused_kernel, n_gr, n_fs, n_tp),
        out_shape=(across, across, down) * 2
        + (jax.ShapeDtypeStruct((owned, depth), jnp.bfloat16),),
        in_specs=[vmem] * 9,
        out_specs=(vmem,) * 7,
        scratch_shapes=[
            pltpu.VMEM((2, tall, cols), jnp.bfloat16),
            pltpu.VMEM((n_tp, owned, depth), jnp.bfloat16),
            pltpu.VMEM((n_tp, owned, depth), jnp.bfloat16),
            pltpu.VMEM((n_tp, owned, width), jnp.bfloat16),
            pltpu.VMEM((2, n_tp // 2, owned, depth), jnp.bfloat16),
            pltpu.VMEM((2, n_tp // 2, owned, depth), jnp.bfloat16),
            pltpu.VMEM((2, n_tp // 2, owned, depth), jnp.bfloat16),
            pltpu.VMEM((2, n_tp // 2, owned, depth), jnp.bfloat16),
            pltpu.VMEM((owned, depth), jnp.float32),
            pltpu.VMEM((owned, depth), jnp.float32),
            dma((2, 3, 2, n_fs)),
            dma((2, 3, 2, n_fs)),
            dma((2, 3, n_gr, n_fs)),
            dma((2, 3, n_gr, n_fs)),
            dma((2, n_gr)),
            dma((2, n_tp)),
            dma((2, n_tp // 2)),
            dma((2, n_tp // 2)),
            dma((2, n_tp // 2)),
            dma((2, n_tp // 2)),
            dma((n_tp - 1,)),
            dma((n_tp - 1,)),
        ],
        compiler_params=pltpu.CompilerParams(
            collective_id=2, has_side_effects=True, vmem_limit_bytes=40 * 2**20
        ),
    )(*operands)
    gate_a, up_a, down_a, gate_b, up_b, down_b = served

    def flat(a):
        return a.reshape(per * tall, n_tp * cols)

    return (gate_a.T, up_a.T, flat(down_a), gate_b.T, up_b.T, flat(down_b), mixed)


def normalize(rows):
    rows = rows.astype(jnp.float32)
    scale = lax.rsqrt(jnp.mean(rows * rows, axis=-1, keepdims=True) + 1e-06)
    return (rows * scale).astype(jnp.bfloat16)


def hidden_units(normed, w_gate, w_up):
    gate = jnp.dot(normed, w_gate, preferred_element_type=jnp.float32)
    upper = jnp.dot(normed, w_up, preferred_element_type=jnp.float32)
    return (jax.nn.silu(gate) * upper).astype(jnp.bfloat16)


def rounded_term(hidden, w_down):
    return jnp.dot(hidden, w_down, preferred_element_type=jnp.float32).astype(jnp.bfloat16)


def shards(
    sizes,
    prompt,
    gain_first,
    gate_first,
    up_first,
    down_first,
    gain_second,
    gate_second,
    up_second,
    down_second,
):
    if gate_first.shape[0] % 128 == 0 and sizes[2] % 2 == 0:
        return fused(
            sizes,
            prompt,
            gain_first,
            gate_first,
            up_first,
            down_first,
            gain_second,
            gate_second,
            up_second,
            down_second,
        )
    gate_a, up_a, down_a = gather(sizes, 0, gain_first, gate_first, up_first, down_first)
    hidden_a = hidden_units(normalize(prompt), gate_a, up_a)
    term_a = rounded_term(hidden_a, down_a)
    term_a, gain_second = lax.optimization_barrier((term_a, gain_second))
    branch_a = lax.psum(term_a, "tp").astype(jnp.float32)
    gate_b, up_b, down_b = gather(sizes, 1, gain_second, gate_second, up_second, down_second)
    stream = prompt.astype(jnp.float32) + 0.5 * branch_a
    hidden_b = hidden_units(normalize(stream), gate_b, up_b)
    owned = hidden_b.shape[0] // lax.axis_size("tp")
    branch_b = lax.psum_scatter(
        rounded_term(hidden_b, down_b), "tp", scatter_dimension=0, tiled=True
    ).astype(jnp.float32)
    own_stream = lax.dynamic_slice_in_dim(stream, lax.axis_index("tp") * owned, owned, 0)
    mixed = (own_stream + 0.5 * branch_b).astype(jnp.bfloat16)
    return (gate_a, up_a, down_a, gate_b, up_b, down_b, mixed)


def solution(mesh):
    sizes = (mesh.shape["gr"], mesh.shape["fs"], mesh.shape["tp"])
    return jax.shard_map(
        functools.partial(shards, sizes),
        mesh=mesh,
        in_specs=(
            P(("gr", "fs"), None),
            P(("gr", "fs")),
            P(("gr", "fs"), "tp"),
            P(("gr", "fs"), "tp"),
            P(("gr", "fs"), "tp"),
            P(("gr", "fs")),
            P(("gr", "fs"), "tp"),
            P(("gr", "fs"), "tp"),
            P(("gr", "fs"), "tp"),
        ),
        out_specs=(
            P(None, "tp"),
            P(None, "tp"),
            P("tp", None),
            P(None, "tp"),
            P(None, "tp"),
            P("tp", None),
            P(("gr", "fs", "tp"), None),
        ),
        check_vma=False,
    )
```

profile of v0, /device:TPU:0, one launch (start us, length us, event | category | flops | bytes accessed | tf_op | source)
XLA Modules:
  0.0 230.7 jit_solution(1275434808466390095)
XLA Ops:
  0.6 219.8 %shard_map.144 = (bf16[704,2048]{1,0:T(8,128)(2,1)S(1)}, bf16[704,2048]{1,0:T(8,128)(2,1)S(1)}, bf16[2,352,2048]{2,1,0:T(8,128)(2,1)S(1)}, bf16[704,2048]{1,0:T(...) custom-call(bf16[4,128,2048]{2,1,0:T(8,128)(2,1)} %bitcast.19, ...), custom_call_target="tpu_custom_call" | custom-call | tf_op jit(solution)/shard_map/pallas_call | solution.py:710
  220.5 1.6 copy.23
  222.1 1.6 copy.24
  223.6 1.6 copy.25
  225.2 1.6 copy.26
  226.8 1.6 copy.27
  228.4 0.0 copy-start
  228.4 1.6 copy.28
  230.0 0.0 copy-done
  230.0 0.8 copy.29
Async XLA Ops:
  228.4 1.6 copy-start
where the time goes:
time: 231 us
  Pallas kernels  220 us (95%)
  local copies, waits for them, and re-layouts  10.3 us (4%)
    pallas_call x1, Pallas kernels, fused(): pl.pallas_call(functools.partial(fused_kernel, n_gr, n_fs, n_tp), out_sha...  220 us
    unnamed x9, local copies, waits for them, and re-layouts  10.3 us

commit v1 on v0

--- a/solution.py
+++ b/solution.py
@@ -282,15 +282,15 @@
     n_gr,
     n_fs,
     n_tp,
-    prompt_ref,
-    gain_a,
-    gate_a,
-    up_a,
-    down_a,
-    gain_b,
-    gate_b,
-    up_b,
-    down_b,
+    prompt_in,
+    gain_in_a,
+    gate_in_a,
+    up_in_a,
+    down_in_a,
+    gain_in_b,
+    gate_in_b,
+    up_in_b,
+    down_in_b,
     gate_out_a,
     up_out_a,
     down_out_a,
@@ -298,14 +298,19 @@
     up_out_b,
     down_out_b,
     mixed_ref,
+    prompt,
+    gains,
+    tall_in,
+    gates_in,
+    load_sem,
     down_own,
     normed,
     normed_all,
     hidden,
-    parts,
+    mate_out,
     mate_in,
     sums,
-    parts_in,
+    sums_in,
     kept,
     stream,
     line_send,
@@ -323,35 +328,47 @@
 ):
     g, f, t = lax.axis_index("gr"), lax.axis_index("fs"), lax.axis_index("tp")
     per = n_gr * n_fs // n_tp
-    cols = down_a.shape[1]
-    width = gate_a.shape[1]
+    tall, cols = down_in_a.shape
+    width = gate_in_a.shape[1]
+    owned, depth = prompt.shape[1], prompt.shape[2]
     first = lax.rem(t * per, n_fs)
     home = (t * per) // n_fs
     row = g * n_fs + f
     owner = row // per
     slot = lax.rem(row, per)
-    half = n_tp * cols // n_gr
-    lane = t * n_gr // n_tp
+    pairs = n_tp // 2
+    seat, core = t // 2, lax.rem(t, 2)
     outs = ((gate_out_a, up_out_a, down_out_a), (gate_out_b, up_out_b, down_out_b))
 
-    def halved(n):
-        return n == 1
-
-    def place(ref, origin):
-        return ref.at[:, pl.ds(pl.multiple_of(origin * width, 128), width)]
-
-    for n, (gain, gate, up, down) in enumerate(
-        ((gain_a, gate_a, up_a, down_a), (gain_b, gate_b, up_b, down_b))
+    half, quarter, eighth = depth // 2, depth // 4, depth // 8
+
+    def lanes(at, size):
+        return pl.ds(pl.multiple_of(at, 128), size)
+
+    def crossed(column, i):
+        return half + column * quarter + i * eighth
+
+    shared = ((0, quarter), (quarter, eighth), (quarter + eighth, eighth))
+    carried = 2 + 2
+    count = carried + len(shared)
+
+    loads = []
+    for k, (src, dst) in enumerate(
+        (
+            (gain_in_a, gains.at[0]),
+            (gate_in_a, gates_in.at[0]),
+            (up_in_a, gates_in.at[1]),
+            (down_in_a, tall_in.at[0]),
+            (prompt_in, prompt),
+            (gain_in_b, gains.at[1]),
+            (down_in_b, tall_in.at[1]),
+            (gate_in_b, gates_in.at[2]),
+            (up_in_b, gates_in.at[3]),
+        )
     ):
-        place(outs[n][0], row)[...] = (gain[...] * gate[...]).astype(jnp.bfloat16)
-        place(outs[n][1], row)[...] = (gain[...] * up[...]).astype(jnp.bfloat16)
-        down_own[n] = down[...].astype(jnp.bfloat16)
-
-        @pl.when(jnp.logical_and(owner == t, lane == g) if halved(n) else owner == t)
-        def _(n=n, down=down):
-            outs[n][2][slot, :, pl.ds(pl.multiple_of(t * cols, 128), cols)] = down[...].astype(
-                jnp.bfloat16
-            )
+        load = pltpu.make_async_copy(src, dst, load_sem.at[k])
+        load.start()
+        loads.append(load)
 
     barrier = pltpu.get_barrier_semaphore()
     for dg in range(n_gr):
@@ -365,7 +382,20 @@
                 )
     for near in (lax.rem(f + 1, n_fs), lax.rem(f + n_fs - 1, n_fs)):
         pl.semaphore_signal(barrier, inc=1, device_id=(g, near, t), device_id_type=MESH)
-    pl.semaphore_wait(barrier, n_gr * n_tp + 1)
+
+    def place(ref, origin):
+        return ref.at[:, pl.ds(pl.multiple_of(origin * width, 128), width)]
+
+    def round_matrix(n, m):
+        place(outs[n][m], row)[...] = (gains[n] * gates_in[2 * n + m]).astype(jnp.bfloat16)
+
+    def round_down(n):
+        rounded = tall_in[n].astype(jnp.bfloat16)
+        down_own[n] = rounded
+
+        @pl.when(owner == t)
+        def _():
+            outs[n][2][slot, :, lanes(t * cols, cols)] = rounded
 
     def held(o):
         return jnp.logical_and(o >= first, o < first + per)
@@ -380,57 +410,59 @@
             device_id_type=MESH,
         )
 
-    def block(n, m, o):
-        if m < 2:
-            return place(outs[n][m], g * n_fs + o)
-        if halved(n):
-            return share_of(n, o, g)
-        return outs[n][2].at[o - first]
-
-    def share_of(n, o, column):
-        return outs[n][2].at[o - first, :, pl.ds(pl.multiple_of(column * half, 128), half)]
-
-    def line(n, m, way, s):
+    def spot(n, p, o, column):
+        if p < 2:
+            return place(outs[n][p], column * n_fs + o)
+        if p < carried:
+            at, size = crossed(column, p - 2), eighth
+        else:
+            at, size = shared[p - carried]
+        return outs[n][2].at[o - first, :, lanes(at, size)]
+
+    def line(n, p, way, s):
         step = 1 if way == 0 else -1
         o = f - step * (s - 1)
-        sems = line_send.at[n, m, way, s], line_recv.at[n, m, way, s]
-        return remote(block(n, m, o), block(n, m, o), *sems, (g, f + step, t))
-
-    def sends(m, way, s):
+        sems = line_send.at[n, p, way, s], line_recv.at[n, p, way, s]
+        return remote(spot(n, p, o, g), spot(n, p, o, g), *sems, (g, f + step, t))
+
+    def sends(p, way, s):
         step = 1 if way == 0 else -1
         o = f - step * (s - 1)
         fine = (f < n_fs - 1, o >= 0) if way == 0 else (f > 0, o <= n_fs - 1)
         ok = jnp.logical_and(*fine)
-        return jnp.logical_and(ok, held(o)) if m == 2 else ok
-
-    def gets(m, way, s):
-        o = f - s if way == 0 else f + s
+        return jnp.logical_and(ok, held(o)) if p >= 2 else ok
+
+    def origin(way, s):
+        return f - s if way == 0 else f + s
+
+    def gets(p, way, s):
+        o = origin(way, s)
         ok = o >= 0 if way == 0 else o <= n_fs - 1
-        return jnp.logical_and(ok, held(o)) if m == 2 else ok
-
-    def landed(n, m, way, s):
-        o = f - s if way == 0 else f + s
-        sems = line_send.at[n, m, way, s], line_recv.at[n, m, way, s]
-        return remote(block(n, m, o), block(n, m, o), *sems, (g, f, t))
-
-    def pair(n, m, dg, o):
-        spot = share_of(n, o, g) if m == 2 else place(outs[n][m], g * n_fs + o)
-        sems = pair_send.at[n, m, dg, o], pair_recv.at[n, m, dg, o]
-        return remote(spot, spot, *sems, (lax.rem(g + dg, n_gr), f, t))
-
-    def pair_landed(n, m, dg, o):
-        src = lax.rem(g - dg + n_gr, n_gr)
-        spot = share_of(n, o, src) if m == 2 else place(outs[n][m], src * n_fs + o)
-        sems = pair_send.at[n, m, dg, o], pair_recv.at[n, m, dg, o]
-        return remote(spot, spot, *sems, (src, f, t))
+        return jnp.logical_and(ok, held(o)) if p >= 2 else ok
+
+    def ends(way):
+        return f == n_fs - 1 if way == 0 else f == 0
+
+    def landed(n, p, way, s):
+        o = origin(way, s)
+        sems = line_send.at[n, p, way, s], line_recv.at[n, p, way, s]
+        return remote(spot(n, p, o, g), spot(n, p, o, g), *sems, (g, f, t))
+
+    def pair(n, p, o):
+        sems = pair_send.at[n, p, o], pair_recv.at[n, p, o]
+        return remote(spot(n, p, o, g), spot(n, p, o, g), *sems, (1 - g, f, t))
+
+    def pair_landed(n, p, o):
+        sems = pair_send.at[n, p, o], pair_recv.at[n, p, o]
+        return remote(spot(n, p, o, 1 - g), spot(n, p, o, 1 - g), *sems, (1 - g, f, t))
 
     def part(n, dg):
         return remote(
             down_own.at[n],
-            outs[n][2].at[slot, :, pl.ds(pl.multiple_of(t * cols, 128), cols)],
+            outs[n][2].at[slot, :, lanes(t * cols, cols)],
             part_send.at[n, dg],
             part_recv.at[n, t],
-            (lane if halved(n) else lax.rem(g + dg, n_gr), f, owner),
+            (lax.rem(g + dg, n_gr), f, owner),
         )
 
     def part_landed(n, src):
@@ -442,254 +474,357 @@
             (home, f, src),
         )
 
-    def start_own(n):
-        for m in range(2):
-            for way in range(2):
-
-                @pl.when(sends(m, way, 1))
-                def _(m=m, way=way):
-                    line(n, m, way, 1).start()
-
-            for dg in range(1, n_gr):
-                pair(n, m, dg, f).start()
-        for dg in range(n_gr):
-            if halved(n):
-                if dg == 0:
-
-                    @pl.when(jnp.logical_or(owner != t, lane != g))
-                    def _():
-                        part(n, 0).start()
-
-            elif dg == 0:
-
-                @pl.when(owner != t)
-                def _():
-                    part(n, 0).start()
-
-            else:
-                part(n, dg).start()
+    def start_lines(n, p):
+        for way in range(2):
+
+            @pl.when(sends(p, way, 1))
+            def _(way=way):
+                line(n, p, way, 1).start()
+
+    def give_part(n):
+        @pl.when(owner != t)
+        def _():
+            part(n, 0).start()
 
     def start_down(n):
         @pl.when(held(f))
         def _():
             for src in range(n_tp):
 
-                away = jnp.logical_or(home != g, t != src)
-                if halved(n):
-                    away = jnp.logical_and(away, g == src * n_gr // n_tp)
-
-                @pl.when(away)
+                @pl.when(jnp.logical_or(home != g, t != src))
                 def _(src=src):
                     part_landed(n, src).wait_recv()
 
-            if halved(n):
-                for dg in range(1, n_gr):
-                    pair(n, 2, dg, f).start()
-
+        for p in range(2, count):
+            start_lines(n, p)
+
+    def forward(n, p, s):
+        crosses, relays = p < carried, s < n_fs - 1
         for way in range(2):
-
-            @pl.when(sends(2, way, 1))
+            if not crosses and not relays:
+                continue
+            ready = gets(p, way, s)
+            if not crosses:
+                ready = jnp.logical_and(ready, jnp.logical_not(ends(way)))
+
+            @pl.when(ready)
             def _(way=way):
-                line(n, 2, way, 1).start()
-
-    def forward(n, m, s):
-        for way in range(2):
-
-            @pl.when(gets(m, way, s))
-            def _(way=way):
-                landed(n, m, way, s).wait_recv()
+                landed(n, p, way, s).wait_recv()
+                if relays:
+
+                    @pl.when(sends(p, way, s + 1))
+                    def _():
+                        line(n, p, way, s + 1).start()
+
+                if crosses:
+                    pair(n, p, origin(way, s)).start()
+
+    def settle(n, p):
+        for s in range(1, n_fs):
+            for way in range(2):
+                ready = gets(p, way, s)
                 if s < n_fs - 1:
-
-                    @pl.when(sends(m, way, s + 1))
-                    def _():
-                        line(n, m, way, s + 1).start()
-
-                if m < 2 or halved(n):
-                    o = f - s if way == 0 else f + s
-                    for dg in range(1, n_gr):
-                        pair(n, m, dg, o).start()
-
-    def pairs_in(n):
-        for m in range(2):
-            for dg in range(1, n_gr):
-                for o in range(n_fs):
-                    pair_landed(n, m, dg, o).wait_recv()
-
-    def halves(n, act):
-        for dg in range(1, n_gr):
+                    ready = jnp.logical_and(ready, ends(way))
+
+                @pl.when(ready)
+                def _(way=way, s=s):
+                    landed(n, p, way, s).wait_recv()
+
+    def pairs_in(n, p):
+        for o in range(n_fs):
+            if p < 2:
+                pair_landed(n, p, o).wait_recv()
+            else:
+
+                @pl.when(jnp.logical_and(held(o), o != f))
+                def _(o=o):
+                    pair_landed(n, p, o).wait_recv()
+
+    def drain(n):
+        for p in range(carried):
             for o in range(n_fs):
-
-                @pl.when(held(o))
-                def _(dg=dg, o=o):
-                    act(n, 2, dg, o)
-
-    def drain(n):
-        if halved(n):
-            halves(n, lambda *at: pair(*at).wait_send())
-        for m in range(2):
-            for dg in range(1, n_gr):
-                for o in range(n_fs):
-                    pair(n, m, dg, o).wait_send()
-        for m in range(3):
+                if p < 2:
+                    pair(n, p, o).wait_send()
+                else:
+
+                    @pl.when(jnp.logical_and(held(o), o != f))
+                    def _(p=p, o=o):
+                        pair(n, p, o).wait_send()
+
+        for p in range(count):
             for way in range(2):
                 for s in range(1, n_fs):
 
-                    @pl.when(sends(m, way, s))
-                    def _(m=m, way=way, s=s):
-                        line(n, m, way, s).wait_send()
-
-        for dg in range(n_gr):
-            if halved(n):
-                if dg == 0:
-
-                    @pl.when(jnp.logical_or(owner != t, lane != g))
-                    def _():
-                        part(n, 0).wait_send()
-
-            elif dg == 0:
-
-                @pl.when(owner != t)
-                def _():
-                    part(n, 0).wait_send()
-
-            else:
-                part(n, dg).wait_send()
-
-    owned, depth = prompt_ref.shape[1], prompt_ref.shape[2]
+                    @pl.when(sends(p, way, s))
+                    def _(p=p, way=way, s=s):
+                        line(n, p, way, s).wait_send()
+
+        @pl.when(owner != t)
+        def _():
+            part(n, 0).wait_send()
+
+        part(n, 1).wait_send()
+
     across = (((1,), (1,)), ((), ()))
 
     def unit(rows):
         return rows * lax.rsqrt(jnp.mean(rows * rows, axis=-1, keepdims=True) + 1e-06)
 
+    def seat_of(j):
+        return lax.rem(seat + 1 + j, pairs)
+
     def hide(n, source):
-        @pl.loop(0, n_tp // 2)
-        def _(i):
-            rows = source[pl.ds(2 * i, 2)].reshape(2 * owned, depth)
+        @pl.loop(0, 2)
+        def _(c):
+            rows = jnp.concatenate([source[c, seat_of(j)] for j in range(pairs)], axis=0)
             gate = lax.dot_general(
                 rows, outs[n][0][...], across, preferred_element_type=jnp.float32
             )
             upper = lax.dot_general(
                 rows, outs[n][1][...], across, preferred_element_type=jnp.float32
             )
-            units = (jax.nn.silu(gate) * upper).astype(jnp.bfloat16)
-            hidden[pl.ds(2 * i, 2)] = units.reshape(2, owned, units.shape[1])
-
-    pairs = n_tp // 2
-    seat, core = t // 2, lax.rem(t, 2)
-
-    def at_seat(j):
-        return 2 * lax.rem(seat + 1 + j, pairs)
-
-    def mate(n, j):
+            hidden[c] = (jax.nn.silu(gate) * upper).astype(jnp.bfloat16)
+
+    ranges = (
+        ((crossed(g, 0), quarter),),
+        ((0, quarter),),
+        ((quarter, eighth), (crossed(1 - g, 0), eighth)),
+        ((quarter + eighth, eighth), (crossed(1 - g, 1), eighth)),
+    )
+    steps = len(ranges)
+    span = depth // steps
+
+    def mate(n, k):
+        at = pl.ds(k * span, span)
         return remote(
-            parts.at[n, j],
-            mate_in.at[n, j],
-            mate_send.at[n, j],
-            mate_recv.at[n, j],
+            mate_out.at[n, :, at],
+            mate_in.at[n, :, at],
+            mate_send.at[n, k],
+            mate_recv.at[n, k],
             (g, f, t + 1 - 2 * core),
         )
 
-    def share(n, j):
+    def share(n, k, j):
+        at = pl.ds(k * span, span)
         return remote(
-            sums.at[n, j],
-            parts_in.at[n, j],
-            sum_send.at[n, j],
-            sum_recv.at[n, j],
-            (g, f, at_seat(j) + core),
-        )
-
-    def term(n, units):
-        tall = outs[n][2].shape[1]
-        total = jnp.zeros((owned, depth), jnp.float32)
-        for k in range(per):
-            total += jnp.dot(
-                units[:, k * tall : (k + 1) * tall],
-                outs[n][2][k],
+            sums.at[n, j, :, at],
+            sums_in.at[n, j, :, at],
+            sum_send.at[n, k, j],
+            sum_recv.at[n, k, j],
+            (g, f, 2 * seat_of(j) + core),
+        )
+
+    def term(n, units, k):
+        tiles = [
+            jnp.dot(
+                units,
+                outs[n][2][:, :, lanes(at, size)].reshape(per * tall, size),
                 preferred_element_type=jnp.float32,
             )
-        return total.astype(jnp.bfloat16)
-
-    def spread(n):
-        for j in range(pairs):
-            parts[n, j] = term(n, hidden[at_seat(j) + 1 - core])
-            if j > 0:
-                mate(n, j - 1).start()
-        for j in range(pairs):
-            mine = term(n, hidden[at_seat(j) + core]).astype(jnp.float32)
-            if j == 0:
-                mate(n, pairs - 1).start()
-            mate(n, j).wait_recv()
-            both = mine + mate_in[n, j].astype(jnp.float32)
-            if j < pairs - 1:
-                sums[n, j] = both.astype(jnp.bfloat16)
-                share(n, j).start()
-            else:
-                kept[...] = both
-
-    def collect(n):
-        total = kept[...]
+            for at, size in ranges[k]
+        ]
+        return tiles[0] if len(tiles) == 1 else jnp.concatenate(tiles, axis=1)
+
+    def offer(n, k):
+        mate_out[n, :, pl.ds(k * span, span)] = term(n, hidden[1 - core], k).astype(jnp.bfloat16)
+        mate(n, k).start()
+
+    def reduce(n, k):
+        at = pl.ds(k * span, span)
+        mine = term(n, hidden[core], k)
+        mate(n, k).wait_recv()
+        both = mine + mate_in[n, :, at].astype(jnp.float32)
         for j in range(pairs - 1):
-            share(n, j).wait_recv()
-            total += parts_in[n, j].astype(jnp.float32)
-        return total
-
-    def give(i):
-        to = lax.rem(t + 1 + i, n_tp)
+            sums[n, j, :, at] = both[j * owned : (j + 1) * owned].astype(jnp.bfloat16)
+            share(n, k, j).start()
+        kept[:, at] = both[(pairs - 1) * owned :]
+
+    def collect(n, k, base, finish):
+        for j in range(pairs - 1):
+            share(n, k, j).wait_recv()
+        total = kept[:, pl.ds(k * span, span)]
+        for j in range(pairs - 1):
+            total += sums_in[n, j, :, pl.ds(k * span, span)].astype(jnp.float32)
+        passed = 0
+        for at, size in ranges[k]:
+            finish(lanes(at, size), base(lanes(at, size)) + 0.5 * total[:, passed : passed + size])
+            passed += size
+
+    def give(j):
+        own = normed_all.at[core, seat]
+        return remote(own, own, row_send.at[j], row_recv.at[j], (g, f, 2 * seat_of(j) + core))
+
+    def given(j):
+        src = lax.rem(seat - 1 - j + pairs, pairs)
+        spot = normed_all.at[core, src]
+        return remote(spot, spot, row_send.at[j], row_recv.at[j], (g, f, 2 * src + core))
+
+    def pass_on(j):
+        src = lax.rem(seat - 1 - j + 2 * pairs, pairs)
+        spot = normed_all.at[core, src]
+        at = pairs - 1 + (pairs - 1 if j < 0 else j)
         return remote(
-            normed_all.at[t], normed_all.at[t], row_send.at[i], row_recv.at[i], (g, f, to)
-        )
-
-    def given(i):
-        src = lax.rem(t - 1 - i + n_tp, n_tp)
+            spot, spot, row_send.at[at], row_recv.at[at], (g, f, t + 1 - 2 * core)
+        )
+
+    def passed_on(j):
+        src = lax.rem(seat - 1 - j + 2 * pairs, pairs)
+        spot = normed_all.at[1 - core, src]
+        at = pairs - 1 + (pairs - 1 if j < 0 else j)
         return remote(
-            normed_all.at[src], normed_all.at[src], row_send.at[i], row_recv.at[i], (g, f, src)
-        )
-
-    start_own(0)
+            spot, spot, row_send.at[at], row_recv.at[at], (g, f, t + 1 - 2 * core)
+        )
+
+    loads[0].wait()
+    loads[1].wait()
+    round_matrix(0, 0)
+    pl.semaphore_wait(barrier, n_gr * n_tp + 1)
+    start_lines(0, 0)
+    pair(0, 0, f).start()
+    loads[2].wait()
+    round_matrix(0, 1)
+    start_lines(0, 1)
+    pair(0, 1, f).start()
+    loads[3].wait()
+    round_down(0)
+    part(0, 1).start()
+    give_part(0)
+    loads[5].wait()
+    loads[6].wait()
+    round_down(1)
+    give_part(1)
+    loads[7].wait()
+    round_matrix(1, 0)
+    loads[8].wait()
+    round_matrix(1, 1)
+    loads[4].wait()
 
     @pl.loop(0, n_tp)
     def _(i):
-        normed[i] = unit(prompt_ref[i].astype(jnp.float32)).astype(jnp.bfloat16)
-
-    start_down(0)
-    for m in range(3):
-        forward(0, m, 1)
-    start_own(1)
+        normed[lax.rem(i, 2), i // 2] = unit(prompt[i].astype(jnp.float32)).astype(jnp.bfloat16)
+
+    def first_half(n):
+        for m in range(2):
+            forward(n, m, 1)
+
+    def second_half(n):
+        for s in range(2, n_fs):
+            for m in range(2):
+                forward(n, m, s)
+            if s == 2:
+                start_down(n)
+
+    def downs(n):
+        for p in range(2, carried):
+            for s in range(1, n_fs):
+                forward(n, p, s)
+        for p in range(carried, count):
+            for s in range(1, n_fs):
+                forward(n, p, s)
+
+    first_half(0)
+    second_half(0)
+    downs(0)
+    part(1, 1).start()
+    for m in range(2):
+        start_lines(1, m)
+        pair(1, m, f).start()
+    for m in range(2):
+        pairs_in(0, m)
+    hide(0, normed)
+    settle(0, carried)
+    offer(0, 0)
+    offer(0, 1)
+    reduce(0, 0)
+    reduce(0, 1)
+    for k in range(2, steps):
+        settle(0, carried + k - 1)
+        pairs_in(0, k)
+        offer(0, k)
+    for k in range(2, steps):
+        reduce(0, k)
+    first_half(1)
+
+    def own_prompt(at):
+        return prompt[t, :, at].astype(jnp.float32)
+
+    def keep_stream(at, value):
+        stream[:, at] = value
+
+    for k in range(steps):
+        collect(0, k, own_prompt, keep_stream)
+    normed_all[core, seat] = unit(stream[...]).astype(jnp.bfloat16)
+    for j in range(pairs - 1):
+        give(j).start()
+    pass_on(-1).start()
     for s in range(2, n_fs):
-        for m in range(3):
-            forward(0, m, s)
-    start_down(1)
-    for m in range(3):
-        forward(1, m, 1)
-    pairs_in(0)
-    hide(0, normed)
-    spread(0)
-    for s in range(2, n_fs - 1):
-        for m in range(3):
+        for m in range(2):
             forward(1, m, s)
-    stream[...] = prompt_ref[t].astype(jnp.float32) + 0.5 * collect(0)
-    normed_all[t] = unit(stream[...]).astype(jnp.bfloat16)
+        if s == 2:
+            start_down(1)
+            for j in range(pairs - 1):
+                given(j).wait_recv()
+                pass_on(j).start()
+    downs(1)
+    for j in range(-1, pairs - 1):
+        passed_on(j).wait_recv()
     for m in range(2):
-        forward(1, m, n_fs - 1)
-    for i in range(n_tp - 1):
-        give(i).start()
-    for i in range(n_tp - 1):
-        given(i).wait_recv()
-    pairs_in(1)
-    forward(1, 2, n_fs - 1)
+        pairs_in(1, m)
     hide(1, normed_all)
-    halves(1, lambda *at: pair_landed(*at).wait_recv())
-    spread(1)
+
+    def keep_mixed(at, value):
+        mixed_ref[:, at] = value.astype(jnp.bfloat16)
+
+    def own_stream(at):
+        return stream[:, at]
+
+    offer(1, 0)
+    settle(1, carried)
+    offer(1, 1)
+    reduce(1, 0)
+    reduce(1, 1)
+    for k in range(2, steps):
+        settle(1, carried + k - 1)
+        pairs_in(1, k)
+        offer(1, k)
+        reduce(1, k)
     drain(0)
     drain(1)
-    mixed_ref[...] = (stream[...] + 0.5 * collect(1)).astype(jnp.bfloat16)
-    for i in range(n_tp - 1):
-        give(i).wait_send()
+    for k in range(steps):
+        collect(1, k, own_stream, keep_mixed)
+    for j in range(pairs - 1):
+        give(j).wait_send()
+    for j in range(-1, pairs - 1):
+        pass_on(j).wait_send()
     for n in range(2):
-        for j in range(pairs):
-            mate(n, j).wait_send()
-            if j < pairs - 1:
-                share(n, j).wait_send()
+        for k in range(steps):
+            mate(n, k).wait_send()
+            for j in range(pairs - 1):
+                share(n, k, j).wait_send()
+
+
+def write_kernel(*refs):
+    count = (len(refs) - 1) // 2
+    sems = refs[-1]
+    copies = [
+        pltpu.make_async_copy(refs[k], refs[count + k], sems.at[k]) for k in range(count)
+    ]
+    for copy in copies:
+        copy.start()
+    for copy in copies:
+        copy.wait()
+
+
+def written(arrays):
+    arrays = [pltpu.with_memory_space_constraint(a, pltpu.VMEM) for a in arrays]
+    return pl.pallas_call(
+        write_kernel,
+        out_shape=tuple(jax.ShapeDtypeStruct(a.shape, a.dtype) for a in arrays),
+        in_specs=[pl.BlockSpec(memory_space=pltpu.VMEM)] * len(arrays),
+        out_specs=(pl.BlockSpec(memory_space=pl.ANY),) * len(arrays),
+        scratch_shapes=[pltpu.SemaphoreType.DMA((len(arrays),))],
+        compiler_params=pltpu.CompilerParams(vmem_limit_bytes=2**20),
+    )(*arrays)
 
 
 def fused(sizes, prompt, *weights):
@@ -699,7 +834,10 @@
     owned = tokens // n_tp
     rows, width = weights[1].shape
     tall, cols = weights[3].shape
+    pairs = n_tp // 2
+    steps, pieces = 4, 7
     vmem = pl.BlockSpec(memory_space=pltpu.VMEM)
+    hbm = pl.BlockSpec(memory_space=pltpu.HBM)
     dma = pltpu.SemaphoreType.DMA
     across = pltpu.VMEM((width, n_gr * n_fs * rows), jnp.bfloat16)
     down = pltpu.VMEM((per, tall, n_tp * cols), jnp.bfloat16)
@@ -707,41 +845,45 @@
     for n in range(2):
         gain, gate, up, tall_block = weights[4 * n : 4 * n + 4]
         operands += [gain[None, :], gate.T, up.T, tall_block]
-    *served, mixed = pl.pallas_call(
+    results = pl.pallas_call(
         functools.partial(fused_kernel, n_gr, n_fs, n_tp),
-        out_shape=(across, across, down) * 2
-        + (jax.ShapeDtypeStruct((owned, depth), jnp.bfloat16),),
-        in_specs=[vmem] * 9,
+        out_shape=(across, across, down) * 2 + (pltpu.VMEM((owned, depth), jnp.bfloat16),),
+        in_specs=[hbm] * 9,
         out_specs=(vmem,) * 7,
         scratch_shapes=[
+            pltpu.VMEM((n_tp, owned, depth), prompt.dtype),
+            pltpu.VMEM((2, 1, rows), jnp.float32),
+            pltpu.VMEM((2, tall, cols), jnp.float32),
+            pltpu.VMEM((4, width, rows), jnp.float32),
+            dma((9,)),
             pltpu.VMEM((2, tall, cols), jnp.bfloat16),
-            pltpu.VMEM((n_tp, owned, depth), jnp.bfloat16),
-            pltpu.VMEM((n_tp, owned, depth), jnp.bfloat16),
-            pltpu.VMEM((n_tp, owned, width), jnp.bfloat16),
-            pltpu.VMEM((2, n_tp // 2, owned, depth), jnp.bfloat16),
-            pltpu.VMEM((2, n_tp // 2, owned, depth), jnp.bfloat16),
-            pltpu.VMEM((2, n_tp // 2, owned, depth), jnp.bfloat16),
-            pltpu.VMEM((2, n_tp // 2, owned, depth), jnp.bfloat16),
+            pltpu.VMEM((2, pairs, owned, depth), jnp.bfloat16),
+            pltpu.VMEM((2, pairs, owned, depth), jnp.bfloat16),
+            pltpu.VMEM((2, pairs * owned, width), jnp.bfloat16),
+            pltpu.VMEM((2, pairs * owned, depth), jnp.bfloat16),
+            pltpu.VMEM((2, pairs * owned, depth), jnp.bfloat16),
+            pltpu.VMEM((2, pairs - 1, owned, depth), jnp.bfloat16),
+            pltpu.VMEM((2, pairs - 1, owned, depth), jnp.bfloat16),
             pltpu.VMEM((owned, depth), jnp.float32),
             pltpu.VMEM((owned, depth), jnp.float32),
-            dma((2, 3, 2, n_fs)),
-            dma((2, 3, 2, n_fs)),
-            dma((2, 3, n_gr, n_fs)),
-            dma((2, 3, n_gr, n_fs)),
+            dma((2, pieces, 2, n_fs)),
+            dma((2, pieces, 2, n_fs)),
+            dma((2, 4, n_fs)),
+            dma((2, 4, n_fs)),
             dma((2, n_gr)),
             dma((2, n_tp)),
-            dma((2, n_tp // 2)),
-            dma((2, n_tp // 2)),
-            dma((2, n_tp // 2)),
-            dma((2, n_tp // 2)),
-            dma((n_tp - 1,)),
-            dma((n_tp - 1,)),
+            dma((2, steps)),
+            dma((2, steps)),
+            dma((2, steps, pairs - 1)),
+            dma((2, steps, pairs - 1)),
+            dma((2 * pairs - 1,)),
+            dma((2 * pairs - 1,)),
         ],
         compiler_params=pltpu.CompilerParams(
-            collective_id=2, has_side_effects=True, vmem_limit_bytes=40 * 2**20
+            collective_id=2, has_side_effects=True, vmem_limit_bytes=36 * 2**20
         ),
     )(*operands)
-    gate_a, up_a, down_a, gate_b, up_b, down_b = served
+    gate_a, up_a, down_a, gate_b, up_b, down_b, mixed = written(results)
 
     def flat(a):
         return a.reshape(per * tall, n_tp * cols)
@@ -763,6 +905,23 @@
 
 def rounded_term(hidden, w_down):
     return jnp.dot(hidden, w_down, preferred_element_type=jnp.float32).astype(jnp.bfloat16)
+
+
+def suits(sizes, prompt, gate, down):
+    n_gr, n_fs, n_tp = sizes
+    per = n_gr * n_fs // n_tp
+    return (
+        n_gr == 2
+        and n_tp % 2 == 0
+        and per > 0
+        and per * n_tp == n_gr * n_fs
+        and n_fs % per == 0
+        and gate.shape[0] % 128 == 0
+        and down.shape[0] % 16 == 0
+        and down.shape[1] % 128 == 0
+        and prompt.shape[1] % 1024 == 0
+        and prompt.shape[0] % (16 * n_tp) == 0
+    )
 
 
 def shards(
@@ -777,7 +936,7 @@
     up_second,
     down_second,
 ):
-    if gate_first.shape[0] % 128 == 0 and sizes[2] % 2 == 0:
+    if suits(sizes, prompt, gate_first, down_first):
         return fused(
             sizes,
             prompt,

time: 231 us -> 192 us (0.83)
  Pallas kernels: 220 us -> 189 us
  local copies, waits for them, and re-layouts: 10.3 us -> 2.46 us
    pallas_call x1, Pallas kernels: 220 us -> 182 us  [fused(): pl.pallas_call(functools.partial(fused_kernel, n_gr, n_fs, n_tp), out_sha...]
    unnamed x9 -> x6, local copies, waits for them, and re-layouts: 10.3 us -> 2.46 us
    pallas_call x0 -> x1, Pallas kernels: none -> 6.22 us  [written(): pl.pallas_call(write_kernel, out_shape=tuple((jax.ShapeDtypeStruct(a.shap...]
where the time goes in v1:
time: 192 us
  Pallas kernels  189 us (98%)
  local copies, waits for them, and re-layouts  2.46 us (1%)
    pallas_call x1, Pallas kernels, fused(): pl.pallas_call(functools.partial(fused_kernel, n_gr, n_fs, n_tp), out_sha...  182 us
    pallas_call x1, Pallas kernels, written(): pl.pallas_call(write_kernel, out_shape=tuple((jax.ShapeDtypeStruct(a.shap...  6.22 us

profile of v1, /device:TPU:0, one launch (start us, length us, event | category | flops | bytes accessed | tf_op | source)
XLA Modules:
  0.0 191.8 jit_solution(1961737706039395428)
XLA Ops:
  0.6 0.0 copy-start
  0.6 1.1 copy-done
  1.7 0.0 copy-start.1
  1.7 0.7 copy-done.1
  2.4 0.0 copy-start.2
  2.4 0.7 copy-done.2
  3.1 182.4 %shard_map.144 = (bf16[704,2048]{1,0:T(8,128)(2,1)S(1)}, bf16[704,2048]{1,0:T(8,128)(2,1)S(1)}, bf16[2,352,2048]{2,1,0:T(8,128)(2,1)S(1)}, bf16[704,2048]{1,0:T(...) custom-call(bf16[4,128,2048]{2,1,0:T(8,128)(2,1)} %bitcast.16, ...), custom_call_target="tpu_custom_call" | custom-call | tf_op jit(solution)/shard_map/pallas_call | solution.py:848
  185.6 6.2 %shard_map.145 = (bf16[704,2048]{1,0:T(8,128)(2,1)}, bf16[704,2048]{1,0:T(8,128)(2,1)}, bf16[2,352,2048]{2,1,0:T(8,128)(2,1)}, bf16[704,2048]{1,0:T(8,128)(2,1)}...) custom-call(bf16[704,2048]{1,0:T(8,128)(2,1)S(1)} %get-tuple-element.21.refs_0_, ...), custom_call_target="tpu_custom_call" | custom-call | tf_op jit(solution)/shard_map/pallas_call | solution.py:820
Async XLA Ops:
  0.6 1.1 copy-start
  1.7 0.7 copy-start.1
  2.4 0.7 copy-start.2

commit v2 on v1

--- a/solution.py
+++ b/solution.py
@@ -278,6 +278,34 @@
     )
 
 
+def down_pieces(depth):
+    half, quarter, eighth, piece = depth // 2, depth // 4, depth // 8, depth // 16
+    split = ((0, eighth), (eighth, piece), (eighth + piece, piece))
+    shared = (
+        (0, quarter),
+        (quarter, eighth),
+        (quarter + eighth, piece),
+        (half - piece, piece),
+    )
+    groups = (((0,), ()), ((1,), (0,)), ((2,), (1,)), ((3,), (2,)))
+    return split, shared, groups
+
+
+def column_ranges(depth, g):
+    split, shared, groups = down_pieces(depth)
+    half, quarter = depth // 2, depth // 4
+    ranges = [((half + g * quarter, quarter),)]
+    for whole, pieces in groups:
+        ranges.append(
+            tuple(shared[i] for i in whole)
+            + tuple((half + (1 - g) * quarter + split[i][0], split[i][1]) for i in pieces)
+        )
+    return ranges
+
+
+INSIDE = 2
+
+
 def fused_kernel(
     n_gr,
     n_fs,
@@ -298,6 +326,8 @@
     up_out_b,
     down_out_b,
     mixed_ref,
+    late_sums,
+    late_rest,
     prompt,
     gains,
     tall_in,
@@ -340,17 +370,17 @@
     seat, core = t // 2, lax.rem(t, 2)
     outs = ((gate_out_a, up_out_a, down_out_a), (gate_out_b, up_out_b, down_out_b))
 
-    half, quarter, eighth = depth // 2, depth // 4, depth // 8
+    split, shared, groups = down_pieces(depth)
+    half, quarter = depth // 2, depth // 4
+    carried = 2 + len(split)
+    count = carried + len(shared)
 
     def lanes(at, size):
         return pl.ds(pl.multiple_of(at, 128), size)
 
     def crossed(column, i):
-        return half + column * quarter + i * eighth
-
-    shared = ((0, quarter), (quarter, eighth), (quarter + eighth, eighth))
-    carried = 2 + 2
-    count = carried + len(shared)
+        at, size = split[i]
+        return half + column * quarter + at, size
 
     loads = []
     for k, (src, dst) in enumerate(
@@ -414,7 +444,7 @@
         if p < 2:
             return place(outs[n][p], column * n_fs + o)
         if p < carried:
-            at, size = crossed(column, p - 2), eighth
+            at, size = crossed(column, p - 2)
         else:
             at, size = shared[p - carried]
         return outs[n][2].at[o - first, :, lanes(at, size)]
@@ -585,17 +615,15 @@
             )
             hidden[c] = (jax.nn.silu(gate) * upper).astype(jnp.bfloat16)
 
-    ranges = (
-        ((crossed(g, 0), quarter),),
-        ((0, quarter),),
-        ((quarter, eighth), (crossed(1 - g, 0), eighth)),
-        ((quarter + eighth, eighth), (crossed(1 - g, 1), eighth)),
-    )
+    ranges = column_ranges(depth, g)
     steps = len(ranges)
-    span = depth // steps
+    widths = [sum(size for _, size in part) for part in ranges]
+    starts = [sum(widths[:k]) for k in range(steps)]
+    spans = [pl.ds(starts[k], widths[k]) for k in range(steps)]
+    kernel_groups = (range(steps), range(INSIDE))
 
     def mate(n, k):
-        at = pl.ds(k * span, span)
+        at = spans[k]
         return remote(
             mate_out.at[n, :, at],
             mate_in.at[n, :, at],
@@ -605,7 +633,7 @@
         )
 
     def share(n, k, j):
-        at = pl.ds(k * span, span)
+        at = spans[k]
         return remote(
             sums.at[n, j, :, at],
             sums_in.at[n, j, :, at],
@@ -625,26 +653,47 @@
         ]
         return tiles[0] if len(tiles) == 1 else jnp.concatenate(tiles, axis=1)
 
+    def arrive(n, k):
+        whole, pieces = groups[k - 1]
+        for i in whole:
+            settle(n, carried + i)
+        for i in pieces:
+            pairs_in(n, 2 + i)
+
     def offer(n, k):
-        mate_out[n, :, pl.ds(k * span, span)] = term(n, hidden[1 - core], k).astype(jnp.bfloat16)
+        mate_out[n, :, spans[k]] = term(n, hidden[1 - core], k).astype(jnp.bfloat16)
         mate(n, k).start()
 
     def reduce(n, k):
-        at = pl.ds(k * span, span)
+        at = spans[k]
         mine = term(n, hidden[core], k)
         mate(n, k).wait_recv()
         both = mine + mate_in[n, :, at].astype(jnp.float32)
+        if k in kernel_groups[n]:
+            for j in range(pairs - 1):
+                sums[n, j, :, at] = both[j * owned : (j + 1) * owned].astype(jnp.bfloat16)
+                share(n, k, j).start()
+            kept[:, at] = both[(pairs - 1) * owned :]
+            return
+        late = starts[k] - starts[INSIDE]
         for j in range(pairs - 1):
-            sums[n, j, :, at] = both[j * owned : (j + 1) * owned].astype(jnp.bfloat16)
-            share(n, k, j).start()
-        kept[:, at] = both[(pairs - 1) * owned :]
+            late_sums[j, :, pl.ds(late, widths[k])] = both[j * owned : (j + 1) * owned].astype(
+                jnp.bfloat16
+            )
+        passed = (pairs - 1) * owned
+        done = 0
+        for column, size in ranges[k]:
+            late_rest[:, pl.ds(late + done, size)] = (
+                stream[:, lanes(column, size)] + 0.5 * both[passed:, done : done + size]
+            )
+            done += size
 
     def collect(n, k, base, finish):
         for j in range(pairs - 1):
             share(n, k, j).wait_recv()
-        total = kept[:, pl.ds(k * span, span)]
+        total = kept[:, spans[k]]
         for j in range(pairs - 1):
-            total += sums_in[n, j, :, pl.ds(k * span, span)].astype(jnp.float32)
+            total += sums_in[n, j, :, spans[k]].astype(jnp.float32)
         passed = 0
         for at, size in ranges[k]:
             finish(lanes(at, size), base(lanes(at, size)) + 0.5 * total[:, passed : passed + size])
@@ -732,17 +781,12 @@
     for m in range(2):
         pairs_in(0, m)
     hide(0, normed)
-    settle(0, carried)
     offer(0, 0)
-    offer(0, 1)
-    reduce(0, 0)
-    reduce(0, 1)
-    for k in range(2, steps):
-        settle(0, carried + k - 1)
-        pairs_in(0, k)
+    for k in range(1, steps):
+        arrive(0, k)
         offer(0, k)
-    for k in range(2, steps):
-        reduce(0, k)
+        reduce(0, k - 1)
+    reduce(0, steps - 1)
     first_half(1)
 
     def own_prompt(at):
@@ -779,18 +823,17 @@
         return stream[:, at]
 
     offer(1, 0)
-    settle(1, carried)
+    arrive(1, 1)
     offer(1, 1)
     reduce(1, 0)
     reduce(1, 1)
     for k in range(2, steps):
-        settle(1, carried + k - 1)
-        pairs_in(1, k)
+        arrive(1, k)
         offer(1, k)
         reduce(1, k)
     drain(0)
     drain(1)
-    for k in range(steps):
+    for k in kernel_groups[1]:
         collect(1, k, own_stream, keep_mixed)
     for j in range(pairs - 1):
         give(j).wait_send()
@@ -799,8 +842,9 @@
     for n in range(2):
         for k in range(steps):
             mate(n, k).wait_send()
-            for j in range(pairs - 1):
-                share(n, k, j).wait_send()
+            if k in kernel_groups[n]:
+                for j in range(pairs - 1):
+                    share(n, k, j).wait_send()
 
 
 def write_kernel(*refs):
@@ -824,7 +868,37 @@
         out_specs=(pl.BlockSpec(memory_space=pl.ANY),) * len(arrays),
         scratch_shapes=[pltpu.SemaphoreType.DMA((len(arrays),))],
         compiler_params=pltpu.CompilerParams(vmem_limit_bytes=2**20),
+        cost_estimate=pl.CostEstimate(
+            flops=2 * 10**9, bytes_accessed=32 * 2**20, transcendentals=0
+        ),
     )(*arrays)
+
+
+def finish_kernel(early_ref, rest_ref, *refs):
+    mixed_ref = refs[-1]
+    depth = early_ref.shape[1]
+    total = rest_ref[...]
+    for received in refs[:-1]:
+        total += 0.5 * received[...].astype(jnp.float32)
+    total = total.astype(mixed_ref.dtype)
+    ranges = column_ranges(depth, lax.axis_index("gr"))
+    done = 0
+    for k, columns in enumerate(ranges):
+        for at, size in columns:
+            at = pl.ds(pl.multiple_of(at, 128), size)
+            if k < INSIDE:
+                mixed_ref[:, at] = early_ref[:, at]
+            else:
+                mixed_ref[:, at] = total[:, done : done + size]
+                done += size
+
+
+def finished(early, rest, received):
+    return pl.pallas_call(
+        finish_kernel,
+        out_shape=jax.ShapeDtypeStruct(early.shape, early.dtype),
+        compiler_params=pltpu.CompilerParams(vmem_limit_bytes=4 * 2**20),
+    )(early, rest, *received)
 
 
 def fused(sizes, prompt, *weights):
@@ -835,7 +909,9 @@
     rows, width = weights[1].shape
     tall, cols = weights[3].shape
     pairs = n_tp // 2
-    steps, pieces = 4, 7
+    split, shared, groups = down_pieces(depth)
+    steps, pieces = 1 + len(groups), 2 + len(split) + len(shared)
+    late = sum(size for columns in column_ranges(depth, 0)[INSIDE:] for _, size in columns)
     vmem = pl.BlockSpec(memory_space=pltpu.VMEM)
     hbm = pl.BlockSpec(memory_space=pltpu.HBM)
     dma = pltpu.SemaphoreType.DMA
@@ -847,9 +923,14 @@
         operands += [gain[None, :], gate.T, up.T, tall_block]
     results = pl.pallas_call(
         functools.partial(fused_kernel, n_gr, n_fs, n_tp),
-        out_shape=(across, across, down) * 2 + (pltpu.VMEM((owned, depth), jnp.bfloat16),),
+        out_shape=(across, across, down) * 2
+        + (
+            pltpu.VMEM((owned, depth), jnp.bfloat16),
+            pltpu.VMEM((pairs - 1, owned, late), jnp.bfloat16),
+            pltpu.VMEM((owned, late), jnp.float32),
+        ),
         in_specs=[hbm] * 9,
-        out_specs=(vmem,) * 7,
+        out_specs=(vmem,) * 9,
         scratch_shapes=[
             pltpu.VMEM((n_tp, owned, depth), prompt.dtype),
             pltpu.VMEM((2, 1, rows), jnp.float32),
@@ -868,8 +949,8 @@
             pltpu.VMEM((owned, depth), jnp.float32),
             dma((2, pieces, 2, n_fs)),
             dma((2, pieces, 2, n_fs)),
-            dma((2, 4, n_fs)),
-            dma((2, 4, n_fs)),
+            dma((2, 2 + len(split), n_fs)),
+            dma((2, 2 + len(split), n_fs)),
             dma((2, n_gr)),
             dma((2, n_tp)),
             dma((2, steps)),
@@ -880,10 +961,18 @@
             dma((2 * pairs - 1,)),
         ],
         compiler_params=pltpu.CompilerParams(
-            collective_id=2, has_side_effects=True, vmem_limit_bytes=36 * 2**20
+            collective_id=2, has_side_effects=True, vmem_limit_bytes=44 * 2**20
         ),
     )(*operands)
-    gate_a, up_a, down_a, gate_b, up_b, down_b, mixed = written(results)
+    *served, early, sums, rest = results
+    received = [
+        lax.ppermute(
+            sums[j], "tp", [(t, (t + 2 * (1 + j)) % n_tp) for t in range(n_tp)]
+        )
+        for j in range(pairs - 1)
+    ]
+    gate_a, up_a, down_a, gate_b, up_b, down_b = written(served)
+    mixed = finished(early, rest, received)
 
     def flat(a):
         return a.reshape(per * tall, n_tp * cols)
@@ -919,7 +1008,7 @@
         and gate.shape[0] % 128 == 0
         and down.shape[0] % 16 == 0
         and down.shape[1] % 128 == 0
-        and prompt.shape[1] % 1024 == 0
+        and prompt.shape[1] % 2048 == 0
         and prompt.shape[0] % (16 * n_tp) == 0
     )
 

time: 192 us -> 186 us (0.969)
  Pallas kernels: 189 us -> 184 us
  local copies, waits for them, and re-layouts: 2.46 us -> 0 us
    pallas_call x1, Pallas kernels: 182 us -> 177 us  [fused(): pl.pallas_call(functools.partial(fused_kernel, n_gr, n_fs, n_tp), out_sha...]
    unnamed x6 -> x0, local copies, waits for them, and re-layouts: 2.46 us -> none
  transfers between devices with their start and end apart: 0 -> 1, of which waited for: 0 -> 1; matrix products, arithmetic and copies ran while one was open for 0% -> 0% of each run, Pallas kernels for 0% -> 3%
where the time goes in v2:
time: 186 us
  Pallas kernels  184 us (99%)
    pallas_call x1, Pallas kernels, fused(): pl.pallas_call(functools.partial(fused_kernel, n_gr, n_fs, n_tp), out_sha...  177 us
    pallas_call x1, Pallas kernels, written(): pl.pallas_call(write_kernel, out_shape=tuple((jax.ShapeDtypeStruct(a.shap...  6.13 us
  transfers between devices with their start and end apart: 1, of which 1 were waited for; matrix products, arithmetic and copies ran while one was open for 0% of the time, Pallas kernels for 3%

profile of v2, /device:TPU:0, one launch (start us, length us, event | category | flops | bytes accessed | tf_op | source)
XLA Modules:
  0.0 186.0 jit_solution(17279399698975474225)
XLA Ops:
  0.6 177.4 %shard_map.144 = (bf16[704,2048]{1,0:T(8,128)(2,1)S(1)}, bf16[704,2048]{1,0:T(8,128)(2,1)S(1)}, bf16[2,352,2048]{2,1,0:T(8,128)(2,1)S(1)}, bf16[704,2048]{1,0:T(...) custom-call(bf16[4,128,2048]{2,1,0:T(8,128)(2,1)} %bitcast.15, ...), custom_call_target="tpu_custom_call" | custom-call | tf_op jit(solution)/shard_map/pallas_call | solution.py:924
  178.0 0.6 collective-permute-start
  178.6 6.1 %shard_map.145 = (bf16[704,2048]{1,0:T(8,128)(2,1)}, bf16[704,2048]{1,0:T(8,128)(2,1)}, bf16[2,352,2048]{2,1,0:T(8,128)(2,1)}, bf16[704,2048]{1,0:T(8,128)(2,1)}...) custom-call(bf16[704,2048]{1,0:T(8,128)(2,1)S(1)} %get-tuple-element.22.refs_0_, ...), custom_call_target="tpu_custom_call" | custom-call | flops 2000000000 | bytes 33554432 | tf_op jit(solution)/shard_map/pallas_call | solution.py:864
  184.7 0.4 collective-permute-done.refs_0_
  185.1 0.9 shard_map.146
Async XLA Ops:
  178.0 7.1 %collective-permute-start = (bf16[128,1024]{1,0:T(8,128)(2,1)S(1)}, bf16[128,1024]{1,0:T(8,128)(2,1)S(1)}, u32[]{:S(2)}, u32[]{:S(2)}) collective-permute-start(bf16[128,1024]{1,0:T(8,128)(2,1)S(1)} %bitcast.14), channel_id=1, source_target_pairs={{0,2},{1,3},{2,0},{3,1},{4,6},{5,7},{6,4},{7,5},{8,10},{9,11},{10,... | collective-permute-start | bytes 786440 | tf_op jit(solution)/shard_map/ppermute | solution.py:969

commit v3 on v2

--- a/solution.py
+++ b/solution.py
@@ -278,28 +278,31 @@
     )
 
 
-def down_pieces(depth):
-    half, quarter, eighth, piece = depth // 2, depth // 4, depth // 8, depth // 16
-    split = ((0, eighth), (eighth, piece), (eighth + piece, piece))
-    shared = (
-        (0, quarter),
-        (quarter, eighth),
-        (quarter + eighth, piece),
-        (half - piece, piece),
-    )
-    groups = (((0,), ()), ((1,), (0,)), ((2,), (1,)), ((3,), (2,)))
-    return split, shared, groups
-
-
-def column_ranges(depth, g):
-    split, shared, groups = down_pieces(depth)
-    half, quarter = depth // 2, depth // 4
-    ranges = [((half + g * quarter, quarter),)]
-    for whole, pieces in groups:
-        ranges.append(
-            tuple(shared[i] for i in whole)
-            + tuple((half + (1 - g) * quarter + split[i][0], split[i][1]) for i in pieces)
-        )
+SPLIT = ((3,), (3, 1, 1))
+SHARED = ((5, 5), (3, 2, 1))
+GROUPS = (
+    (((0,), ()), ((1,), (0,))),
+    (((0,), ()), ((1,), (0,)), ((2,), (1, 2))),
+)
+
+
+def laid(start, sizes):
+    return tuple((start + sum(sizes[:i]), size) for i, size in enumerate(sizes))
+
+
+def down_pieces(n, depth, column):
+    unit = depth // 16
+    split = [unit * size for size in SPLIT[n]]
+    shared = [unit * size for size in SHARED[n]]
+    return laid(sum(shared) + column * sum(split), split), laid(0, shared)
+
+
+def column_ranges(n, depth, g):
+    own, shared = down_pieces(n, depth, g)
+    other, _ = down_pieces(n, depth, 1 - g)
+    ranges = [((own[0][0], sum(size for _, size in own)),)]
+    for whole, pieces in GROUPS[n]:
+        ranges.append(tuple(shared[i] for i in whole) + tuple(other[i] for i in pieces))
     return ranges
 
 
@@ -370,17 +373,11 @@
     seat, core = t // 2, lax.rem(t, 2)
     outs = ((gate_out_a, up_out_a, down_out_a), (gate_out_b, up_out_b, down_out_b))
 
-    split, shared, groups = down_pieces(depth)
-    half, quarter = depth // 2, depth // 4
-    carried = 2 + len(split)
-    count = carried + len(shared)
+    carried = [2 + len(split) for split in SPLIT]
+    count = [c + len(shared) for c, shared in zip(carried, SHARED)]
 
     def lanes(at, size):
         return pl.ds(pl.multiple_of(at, 128), size)
-
-    def crossed(column, i):
-        at, size = split[i]
-        return half + column * quarter + at, size
 
     loads = []
     for k, (src, dst) in enumerate(
@@ -443,16 +440,24 @@
     def spot(n, p, o, column):
         if p < 2:
             return place(outs[n][p], column * n_fs + o)
-        if p < carried:
-            at, size = crossed(column, p - 2)
-        else:
-            at, size = shared[p - carried]
+        split, shared = down_pieces(n, depth, column)
+        at, size = (split + shared)[p - 2]
         return outs[n][2].at[o - first, :, lanes(at, size)]
+
+    def seat_in(n, p, o, most):
+        blocks, downs_before = 2 * n + p, n * (count[0] - 2) + p - 2
+        if p < 2:
+            return blocks * (n_fs + most) + o
+        return 4 * (n_fs + most) + downs_before * (per + most) + o - first
+
+    def line_sems(n, p, way, s, o):
+        own = (n_fs if p < 2 else per + first) if s == 1 and way == 1 else o
+        return line_send.at[seat_in(n, p, own, 1)], line_recv.at[seat_in(n, p, o, 0)]
 
     def line(n, p, way, s):
         step = 1 if way == 0 else -1
         o = f - step * (s - 1)
-        sems = line_send.at[n, p, way, s], line_recv.at[n, p, way, s]
+        sems = line_sems(n, p, way, s, o)
         return remote(spot(n, p, o, g), spot(n, p, o, g), *sems, (g, f + step, t))
 
     def sends(p, way, s):
@@ -475,15 +480,20 @@
 
     def landed(n, p, way, s):
         o = origin(way, s)
-        sems = line_send.at[n, p, way, s], line_recv.at[n, p, way, s]
+        sems = line_sems(n, p, 0, s, o)
         return remote(spot(n, p, o, g), spot(n, p, o, g), *sems, (g, f, t))
 
+    def pair_seat(n, p, o):
+        if p < 2:
+            return (2 * n + p) * n_fs + o
+        return 4 * n_fs + (n * (carried[0] - 2) + p - 2) * per + o - first
+
     def pair(n, p, o):
-        sems = pair_send.at[n, p, o], pair_recv.at[n, p, o]
+        sems = pair_send.at[pair_seat(n, p, o)], pair_recv.at[pair_seat(n, p, o)]
         return remote(spot(n, p, o, g), spot(n, p, o, g), *sems, (1 - g, f, t))
 
     def pair_landed(n, p, o):
-        sems = pair_send.at[n, p, o], pair_recv.at[n, p, o]
+        sems = pair_send.at[pair_seat(n, p, o)], pair_recv.at[pair_seat(n, p, o)]
         return remote(spot(n, p, o, 1 - g), spot(n, p, o, 1 - g), *sems, (1 - g, f, t))
 
     def part(n, dg):
@@ -516,7 +526,7 @@
         def _():
             part(n, 0).start()
 
-    def start_down(n):
+    def parts_in(n):
         @pl.when(held(f))
         def _():
             for src in range(n_tp):
@@ -525,11 +535,8 @@
                 def _(src=src):
                     part_landed(n, src).wait_recv()
 
-        for p in range(2, count):
-            start_lines(n, p)
-
     def forward(n, p, s):
-        crosses, relays = p < carried, s < n_fs - 1
+        crosses, relays = p < carried[n], s < n_fs - 1
         for way in range(2):
             if not crosses and not relays:
                 continue
@@ -571,7 +578,7 @@
                     pair_landed(n, p, o).wait_recv()
 
     def drain(n):
-        for p in range(carried):
+        for p in range(carried[n]):
             for o in range(n_fs):
                 if p < 2:
                     pair(n, p, o).wait_send()
@@ -581,7 +588,7 @@
                     def _(p=p, o=o):
                         pair(n, p, o).wait_send()
 
-        for p in range(count):
+        for p in range(count[n]):
             for way in range(2):
                 for s in range(1, n_fs):
 
@@ -615,15 +622,15 @@
             )
             hidden[c] = (jax.nn.silu(gate) * upper).astype(jnp.bfloat16)
 
-    ranges = column_ranges(depth, g)
-    steps = len(ranges)
-    widths = [sum(size for _, size in part) for part in ranges]
-    starts = [sum(widths[:k]) for k in range(steps)]
-    spans = [pl.ds(starts[k], widths[k]) for k in range(steps)]
-    kernel_groups = (range(steps), range(INSIDE))
+    ranges = [column_ranges(n, depth, g) for n in range(2)]
+    steps = [len(part) for part in ranges]
+    widths = [[sum(size for _, size in columns) for columns in part] for part in ranges]
+    starts = [[sum(sizes[:k]) for k in range(len(sizes))] for sizes in widths]
+    spans = [[pl.ds(*at) for at in zip(starts[n], widths[n])] for n in range(2)]
+    kernel_groups = (range(steps[0]), range(INSIDE))
 
     def mate(n, k):
-        at = spans[k]
+        at = spans[n][k]
         return remote(
             mate_out.at[n, :, at],
             mate_in.at[n, :, at],
@@ -633,7 +640,7 @@
         )
 
     def share(n, k, j):
-        at = spans[k]
+        at = spans[n][k]
         return remote(
             sums.at[n, j, :, at],
             sums_in.at[n, j, :, at],
@@ -649,23 +656,23 @@
                 outs[n][2][:, :, lanes(at, size)].reshape(per * tall, size),
                 preferred_element_type=jnp.float32,
             )
-            for at, size in ranges[k]
+            for at, size in ranges[n][k]
         ]
         return tiles[0] if len(tiles) == 1 else jnp.concatenate(tiles, axis=1)
 
     def arrive(n, k):
-        whole, pieces = groups[k - 1]
+        whole, pieces = GROUPS[n][k - 1]
         for i in whole:
-            settle(n, carried + i)
+            settle(n, carried[n] + i)
         for i in pieces:
             pairs_in(n, 2 + i)
 
     def offer(n, k):
-        mate_out[n, :, spans[k]] = term(n, hidden[1 - core], k).astype(jnp.bfloat16)
+        mate_out[n, :, spans[n][k]] = term(n, hidden[1 - core], k).astype(jnp.bfloat16)
         mate(n, k).start()
 
     def reduce(n, k):
-        at = spans[k]
+        at = spans[n][k]
         mine = term(n, hidden[core], k)
         mate(n, k).wait_recv()
         both = mine + mate_in[n, :, at].astype(jnp.float32)
@@ -675,14 +682,14 @@
                 share(n, k, j).start()
             kept[:, at] = both[(pairs - 1) * owned :]
             return
-        late = starts[k] - starts[INSIDE]
+        late = starts[n][k] - starts[n][INSIDE]
         for j in range(pairs - 1):
-            late_sums[j, :, pl.ds(late, widths[k])] = both[j * owned : (j + 1) * owned].astype(
+            late_sums[j, :, pl.ds(late, widths[n][k])] = both[j * owned : (j + 1) * owned].astype(
                 jnp.bfloat16
             )
         passed = (pairs - 1) * owned
         done = 0
-        for column, size in ranges[k]:
+        for column, size in ranges[n][k]:
             late_rest[:, pl.ds(late + done, size)] = (
                 stream[:, lanes(column, size)] + 0.5 * both[passed:, done : done + size]
             )
@@ -691,11 +698,11 @@
     def collect(n, k, base, finish):
         for j in range(pairs - 1):
             share(n, k, j).wait_recv()
-        total = kept[:, spans[k]]
+        total = kept[:, spans[n][k]]
         for j in range(pairs - 1):
-            total += sums_in[n, j, :, spans[k]].astype(jnp.float32)
+            total += sums_in[n, j, :, spans[n][k]].astype(jnp.float32)
         passed = 0
-        for at, size in ranges[k]:
+        for at, size in ranges[n][k]:
             finish(lanes(at, size), base(lanes(at, size)) + 0.5 * total[:, passed : passed + size])
             passed += size
 
@@ -752,42 +759,49 @@
     def _(i):
         normed[lax.rem(i, 2), i // 2] = unit(prompt[i].astype(jnp.float32)).astype(jnp.bfloat16)
 
-    def first_half(n):
+    def forward_both(n, s):
         for m in range(2):
-            forward(n, m, 1)
-
-    def second_half(n):
-        for s in range(2, n_fs):
-            for m in range(2):
-                forward(n, m, s)
-            if s == 2:
-                start_down(n)
-
-    def downs(n):
-        for p in range(2, carried):
-            for s in range(1, n_fs):
-                forward(n, p, s)
-        for p in range(carried, count):
-            for s in range(1, n_fs):
-                forward(n, p, s)
-
-    first_half(0)
-    second_half(0)
-    downs(0)
+            forward(n, m, s)
+
+    def forward_piece(n, p):
+        for s in range(1, n_fs):
+            forward(n, p, s)
+
+    def spread(n, ks):
+        for i, k in enumerate(ks):
+            if k:
+                arrive(n, k)
+            offer(n, k)
+            if i:
+                reduce(n, ks[i - 1])
+        reduce(n, ks[-1])
+
+    middle = n_fs // 2
+    for s in range(1, middle + 1):
+        forward_both(0, s)
+    parts_in(0)
+    for p in range(2, carried[0] + 1):
+        start_lines(0, p)
+    for s in range(middle + 1, n_fs):
+        forward_both(0, s)
+    for p in range(2, carried[0] + 1):
+        forward_piece(0, p)
     part(1, 1).start()
     for m in range(2):
         start_lines(1, m)
         pair(1, m, f).start()
+    for p in range(carried[0] + 1, count[0]):
+        start_lines(0, p)
+    for p in range(carried[0] + 1, count[0]):
+        forward_piece(0, p)
     for m in range(2):
         pairs_in(0, m)
     hide(0, normed)
-    offer(0, 0)
-    for k in range(1, steps):
-        arrive(0, k)
-        offer(0, k)
-        reduce(0, k - 1)
-    reduce(0, steps - 1)
-    first_half(1)
+    spread(0, range(steps[0] - 1))
+    forward_both(1, 1)
+    spread(0, [steps[0] - 1])
+    for s in range(2, middle + 1):
+        forward_both(1, s)
 
     def own_prompt(at):
         return prompt[t, :, at].astype(jnp.float32)
@@ -795,21 +809,22 @@
     def keep_stream(at, value):
         stream[:, at] = value
 
-    for k in range(steps):
+    for k in range(steps[0]):
         collect(0, k, own_prompt, keep_stream)
     normed_all[core, seat] = unit(stream[...]).astype(jnp.bfloat16)
     for j in range(pairs - 1):
         give(j).start()
     pass_on(-1).start()
-    for s in range(2, n_fs):
-        for m in range(2):
-            forward(1, m, s)
-        if s == 2:
-            start_down(1)
-            for j in range(pairs - 1):
-                given(j).wait_recv()
-                pass_on(j).start()
-    downs(1)
+    parts_in(1)
+    for p in range(2, count[1]):
+        start_lines(1, p)
+    for s in range(middle + 1, n_fs):
+        forward_both(1, s)
+    for j in range(pairs - 1):
+        given(j).wait_recv()
+        pass_on(j).start()
+    for p in range(2, count[1]):
+        forward_piece(1, p)
     for j in range(-1, pairs - 1):
         passed_on(j).wait_recv()
     for m in range(2):
@@ -822,15 +837,9 @@
     def own_stream(at):
         return stream[:, at]
 
-    offer(1, 0)
-    arrive(1, 1)
-    offer(1, 1)
-    reduce(1, 0)
-    reduce(1, 1)
-    for k in range(2, steps):
-        arrive(1, k)
-        offer(1, k)
-        reduce(1, k)
+    spread(1, range(INSIDE))
+    for k in range(INSIDE, steps[1]):
+        spread(1, [k])
     drain(0)
     drain(1)
     for k in kernel_groups[1]:
@@ -840,7 +849,7 @@
     for j in range(-1, pairs - 1):
         pass_on(j).wait_send()
     for n in range(2):
-        for k in range(steps):
+        for k in range(steps[n]):
             mate(n, k).wait_send()
             if k in kernel_groups[n]:
                 for j in range(pairs - 1):
@@ -881,7 +890,7 @@
     for received in refs[:-1]:
         total += 0.5 * received[...].astype(jnp.float32)
     total = total.astype(mixed_ref.dtype)
-    ranges = column_ranges(depth, lax.axis_index("gr"))
+    ranges = column_ranges(1, depth, lax.axis_index("gr"))
     done = 0
     for k, columns in enumerate(ranges):
         for at, size in columns:
@@ -909,9 +918,9 @@
     rows, width = weights[1].shape
     tall, cols = weights[3].shape
     pairs = n_tp // 2
-    split, shared, groups = down_pieces(depth)
-    steps, pieces = 1 + len(groups), 2 + len(split) + len(shared)
-    late = sum(size for columns in column_ranges(depth, 0)[INSIDE:] for _, size in columns)
+    steps = 1 + max(len(groups) for groups in GROUPS)
+    crossing, pieces = sum(map(len, SPLIT)), sum(map(len, SPLIT + SHARED))
+    late = sum(size for columns in column_ranges(1, depth, 0)[INSIDE:] for _, size in columns)
     vmem = pl.BlockSpec(memory_space=pltpu.VMEM)
     hbm = pl.BlockSpec(memory_space=pltpu.HBM)
     dma = pltpu.SemaphoreType.DMA
@@ -947,10 +956,10 @@
             pltpu.VMEM((2, pairs - 1, owned, depth), jnp.bfloat16),
             pltpu.VMEM((owned, depth), jnp.float32),
             pltpu.VMEM((owned, depth), jnp.float32),
-            dma((2, pieces, 2, n_fs)),
-            dma((2, pieces, 2, n_fs)),
-            dma((2, 2 + len(split), n_fs)),
-            dma((2, 2 + len(split), n_fs)),
+            dma((4 * (n_fs + 1) + pieces * (per + 1),)),
+            dma((4 * n_fs + pieces * per,)),
+            dma((4 * n_fs + crossing * per,)),
+            dma((4 * n_fs + crossing * per,)),
             dma((2, n_gr)),
             dma((2, n_tp)),
             dma((2, steps)),

time: 186 us -> 183 us (0.984)
  Pallas kernels: 184 us -> 180 us
    pallas_call x1, Pallas kernels: 177 us -> 173 us  [fused(): pl.pallas_call(functools.partial(fused_kernel, n_gr, n_fs, n_tp), out_sha...]
where the time goes in v3:
time: 183 us
  Pallas kernels  180 us (98%)
    pallas_call x1, Pallas kernels, fused(): pl.pallas_call(functools.partial(fused_kernel, n_gr, n_fs, n_tp), out_sha...  173 us
    pallas_call x1, Pallas kernels, written(): pl.pallas_call(write_kernel, out_shape=tuple((jax.ShapeDtypeStruct(a.shap...  6.13 us
  transfers between devices with their start and end apart: 1, of which 1 were waited for; matrix products, arithmetic and copies ran while one was open for 0% of the time, Pallas kernels for 3%

profile of v3, /device:TPU:0, one launch (start us, length us, event | category | flops | bytes accessed | tf_op | source)
XLA Modules:
  0.0 182.6 jit_solution(3489582016164491036)
XLA Ops:
  0.6 173.0 %shard_map.144 = (bf16[704,2048]{1,0:T(8,128)(2,1)S(1)}, bf16[704,2048]{1,0:T(8,128)(2,1)S(1)}, bf16[2,352,2048]{2,1,0:T(8,128)(2,1)S(1)}, bf16[704,2048]{1,0:T(...) custom-call(bf16[4,128,2048]{2,1,0:T(8,128)(2,1)} %bitcast.15, ...), custom_call_target="tpu_custom_call" | custom-call | tf_op jit(solution)/shard_map/pallas_call | solution.py:933
  173.6 1.5 collective-permute-start
  175.2 6.1 %shard_map.145 = (bf16[704,2048]{1,0:T(8,128)(2,1)}, bf16[704,2048]{1,0:T(8,128)(2,1)}, bf16[2,352,2048]{2,1,0:T(8,128)(2,1)}, bf16[704,2048]{1,0:T(8,128)(2,1)}...) custom-call(bf16[704,2048]{1,0:T(8,128)(2,1)S(1)} %get-tuple-element.22.refs_0_, ...), custom_call_target="tpu_custom_call" | custom-call | flops 2000000000 | bytes 33554432 | tf_op jit(solution)/shard_map/pallas_call | solution.py:873
  181.3 0.4 collective-permute-done.refs_0_
  181.7 0.9 shard_map.146
Async XLA Ops:
  173.6 8.0 %collective-permute-start = (bf16[128,1024]{1,0:T(8,128)(2,1)S(1)}, bf16[128,1024]{1,0:T(8,128)(2,1)S(1)}, u32[]{:S(2)}, u32[]{:S(2)}) collective-permute-start(bf16[128,1024]{1,0:T(8,128)(2,1)S(1)} %bitcast.14), channel_id=1, source_target_pairs={{0,2},{1,3},{2,0},{3,1},{4,6},{5,7},{6,4},{7,5},{8,10},{9,11},{10,... | collective-permute-start | bytes 786440 | tf_op jit(solution)/shard_map/ppermute | solution.py:978

commit v4 on v3

--- a/solution.py
+++ b/solution.py
@@ -279,7 +279,7 @@
 
 
 SPLIT = ((3,), (3, 1, 1))
-SHARED = ((5, 5), (3, 2, 1))
+SHARED = ((5, 5), (4, 1, 1))
 GROUPS = (
     (((0,), ()), ((1,), (0,))),
     (((0,), ()), ((1,), (0,)), ((2,), (1, 2))),
@@ -407,8 +407,14 @@
                     device_id=(lax.rem(g + dg, n_gr), f, lax.rem(t + dt, n_tp)),
                     device_id_type=MESH,
                 )
-    for near in (lax.rem(f + 1, n_fs), lax.rem(f + n_fs - 1, n_fs)):
-        pl.semaphore_signal(barrier, inc=1, device_id=(g, near, t), device_id_type=MESH)
+    for near, there in ((f + 1, f < n_fs - 1), (f - 1, f > 0)):
+
+        @pl.when(there)
+        def _(near=near):
+            pl.semaphore_signal(barrier, inc=1, device_id=(g, near, t), device_id_type=MESH)
+
+    between = jnp.logical_and(f > 0, f < n_fs - 1)
+    greeted = n_gr * n_tp + jnp.where(between, 1, 0)
 
     def place(ref, origin):
         return ref.at[:, pl.ds(pl.multiple_of(origin * width, 128), width)]
@@ -444,15 +450,22 @@
         at, size = (split + shared)[p - 2]
         return outs[n][2].at[o - first, :, lanes(at, size)]
 
-    def seat_in(n, p, o, most):
-        blocks, downs_before = 2 * n + p, n * (count[0] - 2) + p - 2
+    def down_index(n, p):
+        return n * (count[0] - 2) + p - 2
+
+    def send_seat(n, p, o):
         if p < 2:
-            return blocks * (n_fs + most) + o
-        return 4 * (n_fs + most) + downs_before * (per + most) + o - first
+            return 2 * n + p
+        return 4 + down_index(n, p) * (per + 1) + o - first
+
+    def recv_seat(n, p, o):
+        if p < 2:
+            return (2 * n + p) * n_fs + o
+        return 4 * n_fs + down_index(n, p) * per + o - first
 
     def line_sems(n, p, way, s, o):
-        own = (n_fs if p < 2 else per + first) if s == 1 and way == 1 else o
-        return line_send.at[seat_in(n, p, own, 1)], line_recv.at[seat_in(n, p, o, 0)]
+        own = per + first if s == 1 and way == 1 else o
+        return line_send.at[send_seat(n, p, own)], line_recv.at[recv_seat(n, p, o)]
 
     def line(n, p, way, s):
         step = 1 if way == 0 else -1
@@ -485,8 +498,8 @@
 
     def pair_seat(n, p, o):
         if p < 2:
-            return (2 * n + p) * n_fs + o
-        return 4 * n_fs + (n * (carried[0] - 2) + p - 2) * per + o - first
+            return 2 * n + p
+        return 4 + (n * (carried[0] - 2) + p - 2) * per + o - first
 
     def pair(n, p, o):
         sems = pair_send.at[pair_seat(n, p, o)], pair_recv.at[pair_seat(n, p, o)]
@@ -567,28 +580,46 @@
                 def _(way=way, s=s):
                     landed(n, p, way, s).wait_recv()
 
+    def blocks(n, p, origin, many, send, recv):
+        at = pl.ds(pl.multiple_of(origin * width, 128), many * width)
+        spot = outs[n][p].at[:, at]
+        return remote(spot, spot, send, recv, (1 - g, f, t))
+
+    def pair_blocks(n, p, column):
+        sems = pair_send.at[pair_seat(n, p, 0)], pair_recv.at[pair_seat(n, p, 0)]
+        return blocks(n, p, column * n_fs, n_fs, *sems)
+
     def pairs_in(n, p):
+        if p < 2:
+            pair_blocks(n, p, 1 - g).wait_recv()
+            return
         for o in range(n_fs):
-            if p < 2:
+
+            @pl.when(jnp.logical_and(held(o), o != f))
+            def _(o=o):
                 pair_landed(n, p, o).wait_recv()
-            else:
+
+    def drain(n):
+        for p in range(2):
+            pair_blocks(n, p, g).wait_send()
+            sems = line_send.at[send_seat(n, p, 0)], line_recv.at[recv_seat(n, p, 0)]
+
+            @pl.when(between)
+            def _(p=p, sems=sems):
+                blocks(n, p, 0, n_fs + 1, *sems).wait_send()
+
+            @pl.when(jnp.logical_not(between))
+            def _(p=p, sems=sems):
+                blocks(n, p, 0, 1, *sems).wait_send()
+
+        for p in range(2, carried[n]):
+            for o in range(n_fs):
 
                 @pl.when(jnp.logical_and(held(o), o != f))
-                def _(o=o):
-                    pair_landed(n, p, o).wait_recv()
-
-    def drain(n):
-        for p in range(carried[n]):
-            for o in range(n_fs):
-                if p < 2:
+                def _(p=p, o=o):
                     pair(n, p, o).wait_send()
-                else:
-
-                    @pl.when(jnp.logical_and(held(o), o != f))
-                    def _(p=p, o=o):
-                        pair(n, p, o).wait_send()
-
-        for p in range(count[n]):
+
+        for p in range(2, count[n]):
             for way in range(2):
                 for s in range(1, n_fs):
 
@@ -634,7 +665,7 @@
         return remote(
             mate_out.at[n, :, at],
             mate_in.at[n, :, at],
-            mate_send.at[n, k],
+            mate_send.at[n],
             mate_recv.at[n, k],
             (g, f, t + 1 - 2 * core),
         )
@@ -644,7 +675,7 @@
         return remote(
             sums.at[n, j, :, at],
             sums_in.at[n, j, :, at],
-            sum_send.at[n, k, j],
+            sum_send.at[n, j],
             sum_recv.at[n, k, j],
             (g, f, 2 * seat_of(j) + core),
         )
@@ -734,7 +765,7 @@
     loads[0].wait()
     loads[1].wait()
     round_matrix(0, 0)
-    pl.semaphore_wait(barrier, n_gr * n_tp + 1)
+    pl.semaphore_wait(barrier, greeted)
     start_lines(0, 0)
     pair(0, 0, f).start()
     loads[2].wait()
@@ -837,8 +868,7 @@
     def own_stream(at):
         return stream[:, at]
 
-    spread(1, range(INSIDE))
-    for k in range(INSIDE, steps[1]):
+    for k in range(steps[1]):
         spread(1, [k])
     drain(0)
     drain(1)
@@ -849,11 +879,16 @@
     for j in range(-1, pairs - 1):
         pass_on(j).wait_send()
     for n in range(2):
-        for k in range(steps[n]):
-            mate(n, k).wait_send()
-            if k in kernel_groups[n]:
-                for j in range(pairs - 1):
-                    share(n, k, j).wait_send()
+        spot = mate_out.at[n]
+        remote(
+            spot, spot, mate_send.at[n], mate_recv.at[n, 0], (g, f, t + 1 - 2 * core)
+        ).wait_send()
+        whole = pl.ds(0, sum(widths[n][k] for k in kernel_groups[n]))
+        for j in range(pairs - 1):
+            spot = sums.at[n, j, :, whole]
+            remote(
+                spot, spot, sum_send.at[n, j], sum_recv.at[n, 0, j], (g, f, 2 * seat_of(j) + core)
+            ).wait_send()
 
 
 def write_kernel(*refs):
@@ -956,15 +991,15 @@
             pltpu.VMEM((2, pairs - 1, owned, depth), jnp.bfloat16),
             pltpu.VMEM((owned, depth), jnp.float32),
             pltpu.VMEM((owned, depth), jnp.float32),
-            dma((4 * (n_fs + 1) + pieces * (per + 1),)),
+            dma((4 + pieces * (per + 1),)),
             dma((4 * n_fs + pieces * per,)),
-            dma((4 * n_fs + crossing * per,)),
-            dma((4 * n_fs + crossing * per,)),
+            dma((4 + crossing * per,)),
+            dma((4 + crossing * per,)),
             dma((2, n_gr)),
             dma((2, n_tp)),
+            dma((2,)),
             dma((2, steps)),
-            dma((2, steps)),
-            dma((2, steps, pairs - 1)),
+            dma((2, pairs - 1)),
             dma((2, steps, pairs - 1)),
             dma((2 * pairs - 1,)),
             dma((2 * pairs - 1,)),

time: 183 us -> 181 us (0.989)
  no operation moved by 1% of the time
where the time goes in v4:
time: 181 us
  Pallas kernels  179 us (99%)
    pallas_call x1, Pallas kernels, fused(): pl.pallas_call(functools.partial(fused_kernel, n_gr, n_fs, n_tp), out_sha...  172 us
    pallas_call x1, Pallas kernels, written(): pl.pallas_call(write_kernel, out_shape=tuple((jax.ShapeDtypeStruct(a.shap...  6.13 us
  transfers between devices with their start and end apart: 1, of which 1 were waited for; matrix products, arithmetic and copies ran while one was open for 0% of the time, Pallas kernels for 3%

profile of v4, /device:TPU:0, one launch (start us, length us, event | category | flops | bytes accessed | tf_op | source)
XLA Modules:
  0.0 181.3 jit_solution(2822729738506932592)
XLA Ops:
  0.6 171.9 %shard_map.144 = (bf16[704,2048]{1,0:T(8,128)(2,1)S(1)}, bf16[704,2048]{1,0:T(8,128)(2,1)S(1)}, bf16[2,352,2048]{2,1,0:T(8,128)(2,1)S(1)}, bf16[704,2048]{1,0:T(...) custom-call(bf16[4,128,2048]{2,1,0:T(8,128)(2,1)} %bitcast.15, ...), custom_call_target="tpu_custom_call" | custom-call | tf_op jit(solution)/shard_map/pallas_call | solution.py:968
  172.6 1.5 collective-permute-start
  174.1 6.1 %shard_map.145 = (bf16[704,2048]{1,0:T(8,128)(2,1)}, bf16[704,2048]{1,0:T(8,128)(2,1)}, bf16[2,352,2048]{2,1,0:T(8,128)(2,1)}, bf16[704,2048]{1,0:T(8,128)(2,1)}...) custom-call(bf16[704,2048]{1,0:T(8,128)(2,1)S(1)} %get-tuple-element.22.refs_0_, ...), custom_call_target="tpu_custom_call" | custom-call | flops 2000000000 | bytes 33554432 | tf_op jit(solution)/shard_map/pallas_call | solution.py:908
  180.2 0.2 collective-permute-done.refs_0_
  180.4 0.9 shard_map.146
Async XLA Ops:
  172.6 7.8 %collective-permute-start = (bf16[128,896]{1,0:T(8,128)(2,1)S(1)}, bf16[128,896]{1,0:T(8,128)(2,1)S(1)}, u32[]{:S(2)}, u32[]{:S(2)}) collective-permute-start(bf16[128,896]{1,0:T(8,128)(2,1)S(1)} %bitcast.14), channel_id=1, source_target_pairs={{0,2},{1,3},{2,0},{3,1},{4,6},{5,7},{6,4},{7,5},{8,10},{9,11},{10,... | collective-permute-start | bytes 688136 | tf_op jit(solution)/shard_map/ppermute | solution.py:1013

commit v5 on v4

--- a/solution.py
+++ b/solution.py
@@ -278,12 +278,9 @@
     )
 
 
-SPLIT = ((3,), (3, 1, 1))
-SHARED = ((5, 5), (4, 1, 1))
-GROUPS = (
-    (((0,), ()), ((1,), (0,))),
-    (((0,), ()), ((1,), (0,)), ((2,), (1, 2))),
-)
+SPLIT = ((3,), (3, 2))
+SHARED = ((3, 7), (4, 2))
+GROUPS = ((((0,), ()), ((1,), (0,))), (((0,), ()), ((), (0,)), ((1,), (1,))))
 
 
 def laid(start, sizes):
@@ -379,6 +376,25 @@
     def lanes(at, size):
         return pl.ds(pl.multiple_of(at, 128), size)
 
+    barrier = pltpu.get_barrier_semaphore()
+    for dg in range(n_gr):
+        for dt in range(n_tp):
+            if dg or dt:
+                pl.semaphore_signal(
+                    barrier,
+                    inc=1,
+                    device_id=(lax.rem(g + dg, n_gr), f, lax.rem(t + dt, n_tp)),
+                    device_id_type=MESH,
+                )
+    for near, there in ((f + 1, f < n_fs - 1), (f - 1, f > 0)):
+
+        @pl.when(there)
+        def _(near=near):
+            pl.semaphore_signal(barrier, inc=1, device_id=(g, near, t), device_id_type=MESH)
+
+    between = jnp.logical_and(f > 0, f < n_fs - 1)
+    greeted = n_gr * n_tp + jnp.where(between, 1, 0)
+
     loads = []
     for k, (src, dst) in enumerate(
         (
@@ -396,25 +412,6 @@
         load = pltpu.make_async_copy(src, dst, load_sem.at[k])
         load.start()
         loads.append(load)
-
-    barrier = pltpu.get_barrier_semaphore()
-    for dg in range(n_gr):
-        for dt in range(n_tp):
-            if dg or dt:
-                pl.semaphore_signal(
-                    barrier,
-                    inc=1,
-                    device_id=(lax.rem(g + dg, n_gr), f, lax.rem(t + dt, n_tp)),
-                    device_id_type=MESH,
-                )
-    for near, there in ((f + 1, f < n_fs - 1), (f - 1, f > 0)):
-
-        @pl.when(there)
-        def _(near=near):
-            pl.semaphore_signal(barrier, inc=1, device_id=(g, near, t), device_id_type=MESH)
-
-    between = jnp.logical_and(f > 0, f < n_fs - 1)
-    greeted = n_gr * n_tp + jnp.where(between, 1, 0)
 
     def place(ref, origin):
         return ref.at[:, pl.ds(pl.multiple_of(origin * width, 128), width)]
@@ -856,6 +853,7 @@
         pass_on(j).start()
     for p in range(2, count[1]):
         forward_piece(1, p)
+    drain(0)
     for j in range(-1, pairs - 1):
         passed_on(j).wait_recv()
     for m in range(2):
@@ -870,7 +868,6 @@
 
     for k in range(steps[1]):
         spread(1, [k])
-    drain(0)
     drain(1)
     for k in kernel_groups[1]:
         collect(1, k, own_stream, keep_mixed)

time: 181 us -> 181 us (level)
  no operation moved by 1% of the time
where the time goes in v5:
time: 181 us
  Pallas kernels  179 us (99%)
    pallas_call x1, Pallas kernels, fused(): pl.pallas_call(functools.partial(fused_kernel, n_gr, n_fs, n_tp), out_sha...  172 us
    pallas_call x1, Pallas kernels, written(): pl.pallas_call(write_kernel, out_shape=tuple((jax.ShapeDtypeStruct(a.shap...  6.13 us
  transfers between devices with their start and end apart: 1, of which 1 were waited for; matrix products, arithmetic and copies ran while one was open for 0% of the time, Pallas kernels for 3%

profile of v5, /device:TPU:0, one launch (start us, length us, event | category | flops | bytes accessed | tf_op | source)
XLA Modules:
  0.0 180.6 jit_solution(3378258556771705424)
XLA Ops:
  0.6 171.7 %shard_map.144 = (bf16[704,2048]{1,0:T(8,128)(2,1)S(1)}, bf16[704,2048]{1,0:T(8,128)(2,1)S(1)}, bf16[2,352,2048]{2,1,0:T(8,128)(2,1)S(1)}, bf16[704,2048]{1,0:T(...) custom-call(bf16[4,128,2048]{2,1,0:T(8,128)(2,1)} %bitcast.15, ...), custom_call_target="tpu_custom_call" | custom-call | tf_op jit(solution)/shard_map/pallas_call | solution.py:965
  172.3 1.0 collective-permute-start
  173.3 6.1 %shard_map.145 = (bf16[704,2048]{1,0:T(8,128)(2,1)}, bf16[704,2048]{1,0:T(8,128)(2,1)}, bf16[2,352,2048]{2,1,0:T(8,128)(2,1)}, bf16[704,2048]{1,0:T(8,128)(2,1)}...) custom-call(bf16[704,2048]{1,0:T(8,128)(2,1)S(1)} %get-tuple-element.22.refs_0_, ...), custom_call_target="tpu_custom_call" | custom-call | flops 2000000000 | bytes 33554432 | tf_op jit(solution)/shard_map/pallas_call | solution.py:905
  179.4 0.3 collective-permute-done.refs_0_
  179.8 0.9 shard_map.146
Async XLA Ops:
  172.3 7.5 %collective-permute-start = (bf16[128,896]{1,0:T(8,128)(2,1)S(1)}, bf16[128,896]{1,0:T(8,128)(2,1)S(1)}, u32[]{:S(2)}, u32[]{:S(2)}) collective-permute-start(bf16[128,896]{1,0:T(8,128)(2,1)S(1)} %bitcast.14), channel_id=1, source_target_pairs={{0,2},{1,3},{2,0},{3,1},{4,6},{5,7},{6,4},{7,5},{8,10},{9,11},{10,... | collective-permute-start | bytes 688136 | tf_op jit(solution)/shard_map/ppermute | solution.py:1010
